TPU v7x, 128 devices: a whole 4x4x4 slice. The times are simulated.
128 devices in a mesh: ep: 32 (over z, y, core), tp: 4 (over x).
Axes of the slice: x: 4, y: 4, z: 4, core: 2. Of those that a mesh axis runs over, the one named last changes fastest.
Arguments:
- queries: bfloat16 [16384, 1024], P('ep', 'tp'), may hold values from -10.5 to 10.5
- keys: bfloat16 [16384, 512], P('ep', 'tp'), may hold values from -10.5 to 10.5
- values: bfloat16 [16384, 512], P('ep', 'tp'), may hold values from -6 to 6
- head_lambda: float32 [8], P('tp'), may hold values from 0.3 to 0.8
- out_gain: float32 [128], replicated, may hold values from 0.1 to 1.9
- expert_input: bfloat16 [16384, 2048], P(('ep', 'tp')), may hold values from -6 to 6
- routes: int32 [16384, 4], P(('ep', 'tp')), may hold values from 0 to 31, all different within a row; in each aligned block of 128 rows (0 to 127, 128 to 255, ...) at most 20 rows name the same one
- route_weight: float32 [16384, 4], P(('ep', 'tp')), may hold values from 0.2 to 0.6
- moe_gain: float32 [2048], replicated, may hold values from 0.1 to 1.9
- gate_weight: bfloat16 [32, 2048, 2048], P('ep', None, 'tp'), may hold values from -0.3125 to 0.3125
- up_weight: bfloat16 [32, 2048, 2048], P('ep', None, 'tp'), may hold values from -0.3125 to 0.3125
- down_weight: bfloat16 [32, 2048, 2048], P('ep', 'tp'), may hold values from -0.03125 to 0.03125
Outputs:
- mixed_out: bfloat16 [16384, 1024], P('ep', 'tp')
- expert_mix: bfloat16 [16384, 2048], P(('ep', 'tp'))
Inputs may be any that keep to these rules, and one draw needn't show every extreme that they name: `routes`: each row names 4 different experts. Among the rows of one device (aligned blocks of 128 rows) no expert is named more than 20 times, and in some blocks one is named exactly 20 times.
All inputs are finite; a program needn't handle non-finite values.
Results may differ from a plain program's by a relative error of at most 0.012.
Values may be sent and summed in bfloat16 or wider, within the bound.
No kernel may reach another device: no remote copies, remote signals or barrier semaphores. Data moves between devices by JAX's collectives and lax.ppermute only.
A program may use at most 128 MiB of HBM per device.

v0:
```python
import math

import jax
import jax.numpy as jnp
from jax import lax
from jax.sharding import PartitionSpec as P

HEADS = 8
KV_HEADS = 4
HEAD = 64
VDIM = 128


epsilon = 1e-05


def side_by_side(arrays, axis, dim, along):
    ends, at = ([], 0)
    for a in arrays[:-1]:
        at += a.shape[along]
        ends.append(at)
    both = jnp.concatenate(arrays, axis=along)
    return tuple(jnp.split(lax.all_gather(both, axis, axis=dim, tiled=True), ends, axis=along))


def expert_act(rows_in, gate_matrix, up_matrix):
    gate_pre = jnp.dot(rows_in, gate_matrix, preferred_element_type=jnp.float32)
    up_pre = jnp.dot(rows_in, up_matrix, preferred_element_type=jnp.float32)
    clipped = jnp.minimum(gate_pre, 7.0)
    up_clip = jnp.clip(up_pre, -7.0, 7.0)
    return ((up_clip + 1.0) * clipped * jax.nn.sigmoid(1.702 * clipped)).astype(jnp.bfloat16)


def shards(
    queries,
    keys,
    values,
    head_lambda,
    out_gain,
    expert_input,
    routes,
    route_weight,
    moe_gain,
    gate_weight,
    up_weight,
    down_weight,
):
    seq_rows = queries.shape[0]
    kv_local = keys.shape[1] // (2 * HEAD)
    group_size = HEADS // KV_HEADS
    query_start = lax.axis_index("ep") * seq_rows
    score_scale = HEAD ** (-0.5)
    query_sets = [(queries, query_start + jnp.arange(seq_rows, dtype=jnp.int32))]
    set_views = [
        rows.reshape(rows.shape[0], kv_local, group_size, 2, HEAD) for rows, unused in query_sets
    ]
    set_positions = [positions for unused, positions in query_sets]
    set_last = [positions[-1] for positions in set_positions]

    def update(running, query_view, query_pos, key_block, value_block, key_start):
        run_max, run_total, run_sum = running
        scores = (
            jnp.einsum(
                "tkgmd,skmd->mtkgs", query_view, key_block, preferred_element_type=jnp.float32
            )
            * score_scale
        )
        key_pos = key_start + jnp.arange(key_block.shape[0], dtype=jnp.int32)
        allowed = (key_pos[None, :] <= query_pos[:, None])[None, :, None, None, :]
        block_max = jnp.max(jnp.where(allowed, scores, -jnp.inf), axis=-1)
        new_max = jnp.maximum(run_max, block_max)
        weights = jnp.where(allowed, jnp.exp(scores - new_max[..., None]), 0.0)
        factor = jnp.exp(run_max - new_max)
        new_total = factor * run_total + jnp.sum(weights, axis=-1)
        new_sum = factor[..., None] * run_sum + jnp.einsum(
            "ournf,frj->ournj",
            weights.astype(jnp.bfloat16),
            value_block,
            preferred_element_type=jnp.float32,
        )
        return (new_max, new_total, new_sum)

    initial = tuple(
        (
            (
                jnp.full((2, view.shape[0], kv_local, group_size), -1e30, jnp.float32),
                jnp.zeros((2, view.shape[0], kv_local, group_size), jnp.float32),
                jnp.zeros((2, view.shape[0], kv_local, group_size, VDIM), jnp.float32),
            )
            for view in set_views
        )
    )
    key_piece, value_piece = side_by_side((keys, values), "ep", 0, 1)
    piece_rows = key_piece.shape[0]
    block_len = math.gcd(piece_rows, 512)
    key_view = key_piece.reshape(piece_rows, kv_local, 2, HEAD)
    value_view = value_piece.reshape(piece_rows, kv_local, VDIM)

    def block_step(block_index, inner_state):
        offset = block_index * block_len
        key_block = lax.dynamic_slice_in_dim(key_view, offset, block_len, 0)
        value_block = lax.dynamic_slice_in_dim(value_view, offset, block_len, 0)
        set_index = 0

        def compute(current, set_index=set_index):
            return update(
                current,
                set_views[set_index],
                set_positions[set_index],
                key_block,
                value_block,
                offset,
            )

        results = [
            lax.cond(
                offset <= set_last[set_index],
                compute,
                lambda unchanged: unchanged,
                inner_state[set_index],
            )
        ]
        return tuple(results)

    folded = lax.fori_loop(0, piece_rows // block_len, block_step, initial)
    lambdas = head_lambda.reshape(kv_local, group_size)[None, :, :, None]
    finished = []
    for run_max, run_total, run_sum in folded:
        combined = (
            run_sum[0] / run_total[0][..., None] - lambdas * run_sum[1] / run_total[1][..., None]
        )
        inverse_rms = lax.rsqrt(jnp.mean(combined * combined, axis=-1, keepdims=True) + epsilon)
        finished.append(
            (combined * inverse_rms * out_gain)
            .astype(jnp.bfloat16)
            .reshape(combined.shape[0], kv_local * group_size * VDIM)
        )
    mixed_out = finished[0]
    token_count = expert_input.shape[0]
    top_count = routes.shape[1]
    model_width = expert_input.shape[1]
    ep_count = lax.axis_size("ep")
    capacity = 5 * token_count * top_count // (4 * ep_count)
    inputs_f32 = expert_input.astype(jnp.float32)
    normed = (
        inputs_f32
        * lax.rsqrt(jnp.mean(inputs_f32 * inputs_f32, axis=-1, keepdims=True) + epsilon)
        * moe_gain
    ).astype(jnp.bfloat16)
    flat_routes = routes.reshape(-1)
    route_total = flat_routes.shape[0]
    one_hot = (flat_routes[:, None] == jnp.arange(ep_count, dtype=jnp.int32)[None, :]).astype(
        jnp.int32
    )
    slot_rank = jnp.sum(jnp.cumsum(one_hot, axis=0) * one_hot, axis=1) - 1
    target = flat_routes * capacity + slot_rank
    slot_token = (
        jnp.zeros((ep_count * capacity,), jnp.int32)
        .at[target]
        .set(jnp.arange(route_total, dtype=jnp.int32) // top_count)
    )
    slot_live = jnp.zeros((ep_count * capacity,), jnp.bool_).at[target].set(True)
    outgoing = jnp.where(slot_live[:, None], normed[slot_token], jnp.zeros((), jnp.bfloat16))
    local_gate = gate_weight[0]
    local_up = up_weight[0]
    local_down = down_weight[0]
    arrived = lax.all_to_all(outgoing, "ep", split_axis=0, concat_axis=0, tiled=True)
    activated = expert_act(lax.all_gather(arrived, "tp", axis=0, tiled=True), local_gate, local_up)
    summed = lax.psum_scatter(
        jnp.dot(activated, local_down, preferred_element_type=jnp.float32).astype(jnp.bfloat16),
        "tp",
        scatter_dimension=0,
        tiled=True,
    )
    returned = lax.all_to_all(summed, "ep", split_axis=0, concat_axis=0, tiled=True)
    picked = returned[target].reshape(token_count, top_count, model_width).astype(jnp.float32)
    expert_mix = jnp.sum(route_weight[:, :, None] * picked, axis=1).astype(jnp.bfloat16)
    return (mixed_out, expert_mix)


def solution(mesh):
    placed = (
        P("ep", "tp"),
        P("ep", "tp"),
        P("ep", "tp"),
        P("tp"),
        P(),
        P(("ep", "tp"), None),
        P(("ep", "tp"), None),
        P(("ep", "tp"), None),
        P(),
        P("ep", None, "tp"),
        P("ep", None, "tp"),
        P("ep", "tp", None),
    )
    return jax.shard_map(
        shards,
        mesh=mesh,
        in_specs=placed,
        out_specs=(P("ep", "tp"), P(("ep", "tp"), None)),
        check_vma=False,
    )
```

profile of v0, /device:TPU:121, one launch (start us, length us, event | category | flops | bytes accessed | tf_op | source)
XLA Modules:
  0.0 550.6 jit_solution(6554158704012025441)
XLA Ops:
  16.7 4.1 gather_fusion
  20.7 5.2 gather.9
  30.7 44.0 %all_to_all.21 = bf16[32,20,2048]{2,1,0:T(8,128)(2,1)} all-to-all(bf16[32,20,2048]{2,1,0:T(8,128)(2,1)S(1)} %broadcast_select_fusion), channel_id=1, replica_groups=mesh['ep'=32,'tp'=4] {'ep'}, dimensions={0} | all-to-all | bytes 5242880 | tf_op jit(solution)/shard_map/all_to_all | solution.py:167
  74.7 5.2 all_to_all.15
  80.1 100.9 %all-gather.5.cloned.1.call-done = bf16[2560,2048]{1,0:T(8,128)(2,1)} async-done(((bf16[640,2048]{1,0:T(8,128)(2,1)}), bf16[2560,2048]{1,0:T(8,128)(2,1)}) %all-gather.5.cloned.1.call-update) | async-done | bytes 10485776 | tf_op jit(solution)/shard_map/all_gather | solution.py:168
  180.9 10.5 %convolution_clamp_fusion = f32[2560,512]{1,0:T(8,128)} fusion(bf16[2560,2048]{1,0:T(8,128)(2,1)} %all-gather.5.cloned.1.call-done, bf16[1,2048,512]{2,1,0:T(8,128)(2,1)} %param.26), kind=kOutput, calls=%fused_computation.35 | convolution fusion | flops 5370019840 | bytes 17825792 | tf_op jit(solution)/shard_map/dot_general | solution.py:28
  191.4 18.4 %convolution_convert_fusion = bf16[2560,2048]{1,0:T(8,128)(2,1)} fusion(f32[2560,512]{1,0:T(8,128)} %convolution_clamp_fusion, bf16[2560,2048]{1,0:T(8,128)(2,1)} %all-gather.5.cloned.1.call-done, bf16[1,512,2048]{2,1,0:T(8,128)(2,1)S(1)} %copy-done, bf16[1,2048,512]{2,1,0:T(8,128)(2,1)} %param.25), kind=kOutput, calls=%fused_computation.34 | convolution fusion | flops 10754457600 | bytes 30408704 | tf_op jit(solution)/shard_map/dot_general | solution.py:170
  212.7 95.9 %reduce-scatter.2.cloned.1.call-done = bf16[640,2048]{1,0:T(8,128)(2,1)} async-done(((bf16[2560,2048]{1,0:T(8,128)(2,1)}), bf16[640,2048]{1,0:T(8,128)(2,1)}) %reduce-scatter.2.cloned.1.call-update) | async-done | bytes 2621456 | tf_op jit(solution)/shard_map/reduce_scatter | solution.py:169
  308.6 5.2 all_to_all.16
  313.8 7.7 %all-to-all-start.1 = ((bf16[32,20,2048]{2,1,0:T(8,128)(2,1)}), bf16[32,20,2048]{2,1,0:T(8,128)(2,1)}, u32[]{:S(2)}, u32[]{:S(2)}) async-start(bf16[32,20,2048]{2,1,0:T(8,128)(2,1)} %all_to_all.16), calls=%async_computation.2 | async-start | bytes 6291456 | tf_op jit(solution)/shard_map/all_to_all | solution.py:175
  321.6 5.8 %slice_bitcast_fusion = (bf16[16384,1,128]{0,2,1:T(8,128)(2,1)}, bf16[16384,128]{0,1:T(8,128)(2,1)}) fusion(bf16[16384,256]{0,1:T(8,128)(2,1)} %all-gather.3.cloned.1.call-done), kind=kLoop, calls=%fused_computation.37 | loop fusion | bytes 16777216 | tf_op jit(solution)/shard_map/reshape | solution.py:97
  327.6 188.1 %while.18 = (s32[]{:T(128)}, f32[2,512,1,2]{1,3,0,2:T(2,128)S(1)}, f32[2,512,1,2]{1,3,0,2:T(2,128)S(1)}, f32[2,512,1,2,128]{1,4,3,0,2:T(8,128)S(1)}, s32[]{:T(12...) while((s32[]{:T(128)}, f32[2,512,1,2]{1,3,0,2:T(2,128)S(1)}, ...), condition=%wide.region_5.6_spmd.clone, body=%wide.region_0.5_spmd.clone.sunk | while | flops 414981120 | bytes 16396601 | solution.py:125
  328.2 5.3 conditional.3
  334.0 5.3 conditional.3
  339.9 5.3 conditional.3
  345.8 5.3 conditional.3
  351.7 5.3 conditional.3
  357.5 5.3 conditional.3
  363.4 5.3 conditional.3
  369.3 5.3 conditional.3
  375.2 5.3 conditional.3
  381.1 5.3 conditional.3
  386.9 5.3 conditional.3
  392.8 5.3 conditional.3
  398.7 5.3 conditional.3
  404.6 5.3 conditional.3
  410.4 5.3 conditional.3
  416.3 5.3 conditional.3
  422.2 5.3 conditional.3
  428.1 5.3 conditional.3
  434.0 5.3 conditional.3
  439.8 5.3 conditional.3
  445.7 5.3 conditional.3
  451.6 5.3 conditional.3
  457.5 5.3 conditional.3
  463.3 5.3 conditional.3
  469.2 5.3 conditional.3
  475.1 5.3 conditional.3
  481.0 5.3 conditional.3
  486.9 5.3 conditional.3
  492.7 5.3 conditional.3
  498.6 5.3 conditional.3
  504.5 5.3 conditional.3
  510.4 5.3 conditional.3
  519.6 5.2 all_to_all.18
  524.7 7.5 %gather_fusion.1 = bf16[512,2048]{1,0:T(8,128)(2,1)} fusion(bf16[640,2048]{1,0:T(8,128)(2,1)} %all_to_all.18, s32[1024]{0:T(1024)S(1)} %pad_clamp_fusion), kind=kCustom, calls=%fused_computation.1 | custom fusion | bytes 4196352 | tf_op jit(solution)/shard_map/gather | solution.py:176
  532.2 4.8 reshape.254
  537.0 6.2 %multiply_reduce_fusion = bf16[128,2048]{1,0:T(8,128)(2,1)} fusion(f32[128,4,2048]{2,1,0:T(4,128)} %reshape.254, f32[128,4]{1,0:T(8,128)S(1)} %copy.49), kind=kLoop, calls=%fused_computation.38 | loop fusion | flops 1835008 | bytes 4720640 | tf_op jit(solution)/shard_map/reduce_sum | solution.py:177
  (364 shorter events, 187.2 us)
Async XLA Ops:
  8.0 183.4 %copy-start = (bf16[1,512,2048]{2,1,0:T(8,128)(2,1)S(1)}, bf16[1,512,2048]{2,1,0:T(8,128)(2,1)}, u32[]{:S(2)}) copy-start(bf16[1,512,2048]{2,1,0:T(8,128)(2,1)} %param.27) | copy-start | bytes 6291460
  8.0 172.9 %all-gather.5.cloned.1.call-start = ((), (), s32[]{:S(2)}) async-start(), calls=%async_computation.4 | async-start | bytes 13107200 | tf_op jit(solution)/shard_map/all_gather | solution.py:168
  79.9 228.8 %reduce-scatter.2.cloned.1.call-start = ((), (), s32[]{:S(2)}) async-start(), calls=%async_computation.5 | async-start | bytes 13107200 | tf_op jit(solution)/shard_map/reduce_scatter | solution.py:169
  209.9 0.9 copy-start.3
  209.9 1.0 copy-start.4
  209.9 2.5 copy-start.2
  209.9 2.7 copy-start.6
  209.9 2.8 copy-start.5
  209.9 2.8 copy-start.7
  209.9 111.7 %all-gather.3.cloned.1.call-start = ((), (), s32[]{:S(2)}) async-start(), calls=%async_computation.3 | async-start | bytes 8650752 | tf_op jit(solution)/shard_map/all_gather | solution.py:23
  313.8 205.7 %all-to-all-start.1 = ((bf16[32,20,2048]{2,1,0:T(8,128)(2,1)}), bf16[32,20,2048]{2,1,0:T(8,128)(2,1)}, u32[]{:S(2)}, u32[]{:S(2)}) async-start(bf16[32,20,2048]{2,1,0:T(8,128)(2,1)} %all_to_all.16), calls=%async_computation.2 | async-start | bytes 6291456 | tf_op jit(solution)/shard_map/all_to_all | solution.py:175
  524.7 18.5 %copy-start.1 = (bf16[1,512,2048]{2,1,0:T(8,128)(2,1)S(1)}, bf16[1,512,2048]{2,1,0:T(8,128)(2,1)}, u32[]{:S(2)}) copy-start(bf16[1,512,2048]{2,1,0:T(8,128)(2,1)} %param.27) | copy-start | bytes 6291460
Sparse Core Ops, SparseCore 0:
  80.0 100.9 all-gather.4
  210.1 98.5 reduce-scatter.1
Sparse Core Ops, SparseCore 1:
  213.2 58.0 all-gather.2
where the time goes:
time: 553 us; the launch traced here: 551 us
  waiting for transfers between devices  197 us (36%)
  matrix products  158 us (29%)
  local copies, waits for them, and re-layouts  54.4 us (10%)
  other arithmetic  52.5 us (9%)
  blocking collectives  44 us (8%)
  loops' own time  21.2 us (4%)
  between operations  15.8 us (3%)
  starting transfers between devices  8.05 us (1%)
    all_gather x1, waiting for transfers between devices, shards(): lax.all_gather(arrived, 'tp', axis=0, tiled=True)  101 us
    reduce_scatter x1, waiting for transfers between devices, shards(): lax.psum_scatter(jnp.dot(activated, local_down, preferred_element_type=jn...  95.9 us
    dot_general x32, matrix products, update(): jnp.einsum('ournf,frj->ournj', weights.astype(jnp.bfloat16), value_block,...  72 us
    dot_general x32, matrix products, update(): jnp.einsum('tkgmd,skmd->mtkgs', query_view, key_block, preferred_element_...  57 us
    all_to_all x1, blocking collectives, shards(): lax.all_to_all(outgoing, 'ep', split_axis=0, concat_axis=0, tiled=True)  44 us
    reduce_sum x32, other arithmetic, update(): new_total = factor * run_total + jnp.sum(weights, axis=-1)  29.6 us
    another operation x1, loops' own time, shards(): folded = lax.fori_loop(0, piece_rows // block_len, block_step, initial)  19 us
    dot_general x1, matrix products, shards(): jnp.dot(activated, local_down, preferred_element_type=jnp.float32)  18.4 us
  transfers between devices with their start and end apart: 4, of which 2 were waited for; matrix products, arithmetic and copies ran while one was open for 32% of the time, Pallas kernels for 0%

commit v1 on v0

v1 whole, which is shorter than its diff:
```python
import functools

import jax
import jax.numpy as jnp
from jax import lax
from jax.experimental import pallas as pl
from jax.experimental.pallas import tpu as pltpu
from jax.sharding import PartitionSpec as P

HEADS = 8
KV_HEADS = 4
HEAD = 64
VDIM = 128
LOG2E = 1.4426950408889634
KEY_BLOCK = 1024
CHUNKS = ((0, 4), (4, 8), (12, 8))

epsilon = 1e-05


def attention_kernel(start_ref, lambda_ref, gain_ref, query_ref, key_ref, value_ref, out_ref, max_ref, sum_ref):
    group = pl.program_id(0)
    start = start_ref[group]
    rows = query_ref.shape[1]
    lane = lax.broadcasted_iota(jnp.int32, (rows, 2 * HEAD), 1)
    max_ref[...] = jnp.full(max_ref.shape, -1e30, jnp.float32)
    sum_ref[...] = jnp.zeros(sum_ref.shape, jnp.float32)
    ones = jnp.ones((KEY_BLOCK, VDIM), jnp.bfloat16)

    def one_block(offset, masked):
        keys = key_ref[pl.ds(offset, KEY_BLOCK), :]
        values = jnp.concatenate([value_ref[pl.ds(offset, KEY_BLOCK), :], ones], axis=1)
        if masked:
            column = lax.broadcasted_iota(jnp.int32, (rows, KEY_BLOCK), 1) + offset
            row = lax.broadcasted_iota(jnp.int32, (rows, KEY_BLOCK), 0) + start
            allowed = column <= row
        for which in range(4):
            mapped, head = which // 2, which % 2
            query = query_ref[0, :, head * 2 * HEAD:(head + 1) * 2 * HEAD]
            query = jnp.where((lane // HEAD) == mapped, query, jnp.zeros((), jnp.bfloat16)) * jnp.bfloat16(HEAD ** -0.5)
            scores = lax.dot_general(query, keys, (((1,), (1,)), ((), ())), preferred_element_type=jnp.float32)
            if masked:
                scores = jnp.where(allowed, scores, -1e30)
            old_max = max_ref[which]
            new_max = jnp.maximum(old_max, jnp.max(scores, axis=-1, keepdims=True))
            factor = jnp.exp2((old_max - new_max) * LOG2E)
            weights = jnp.exp2((scores - new_max) * LOG2E).astype(jnp.bfloat16)
            summed = jnp.dot(weights, values, preferred_element_type=jnp.float32)
            sum_ref[which] = factor * sum_ref[which] + summed
            max_ref[which] = new_max

    whole = start // KEY_BLOCK

    def step(index, carry):
        one_block(pl.multiple_of(index * KEY_BLOCK, KEY_BLOCK), False)
        return carry

    lax.fori_loop(0, whole, step, 0)
    one_block(pl.multiple_of(whole * KEY_BLOCK, KEY_BLOCK), True)
    for head in range(2):
        first, second = sum_ref[head], sum_ref[2 + head]
        combined = first[:, :VDIM] / first[:, VDIM:] - lambda_ref[head] * (second[:, :VDIM] / second[:, VDIM:])
        inverse = lax.rsqrt(jnp.mean(combined * combined, axis=-1, keepdims=True) + epsilon)
        out_ref[0, :, head * VDIM:(head + 1) * VDIM] = (combined * inverse * gain_ref[...]).astype(jnp.bfloat16)


def attention(starts, head_lambda, out_gain, query_sets, keys, values):
    groups, rows, width = query_sets.shape
    length = keys.shape[0]
    return pl.pallas_call(
        attention_kernel,
        grid=(groups,),
        in_specs=[
            pl.BlockSpec(memory_space=pltpu.SMEM),
            pl.BlockSpec(memory_space=pltpu.SMEM),
            pl.BlockSpec((1, VDIM), lambda g: (0, 0)),
            pl.BlockSpec((1, rows, width), lambda g: (g, 0, 0)),
            pl.BlockSpec((length, 2 * HEAD), lambda g: (0, 0)),
            pl.BlockSpec((length, VDIM), lambda g: (0, 0)),
        ],
        out_specs=pl.BlockSpec((1, rows, width), lambda g: (g, 0, 0)),
        out_shape=jax.ShapeDtypeStruct((groups, rows, width), jnp.bfloat16),
        scratch_shapes=[
            pltpu.VMEM((4, rows, 1), jnp.float32),
            pltpu.VMEM((4, rows, 2 * VDIM), jnp.float32),
        ],
        compiler_params=pltpu.CompilerParams(vmem_limit_bytes=48 * 1024 * 1024),
        cost_estimate=pl.CostEstimate(flops=18_000_000_000, transcendentals=18_000_000, bytes_accessed=9_000_000),
        name="attention",
    )(starts, head_lambda, out_gain, query_sets, keys, values)


def dispatch_kernel(routes_ref, input_ref, gain_ref, *out_refs):
    tokens = input_ref.shape[0]
    values = input_ref[...].astype(jnp.float32)
    inverse = lax.rsqrt(jnp.mean(values * values, axis=-1, keepdims=True) + epsilon)
    normed = (values * inverse * gain_ref[...]).astype(jnp.bfloat16)
    expert = lax.broadcasted_iota(jnp.int32, (tokens, tokens), 0)
    other = lax.broadcasted_iota(jnp.int32, (tokens, tokens), 1)
    chosen = jnp.zeros((tokens, tokens), jnp.float32)
    for k in range(routes_ref.shape[0]):
        chosen = chosen + jnp.where(routes_ref[k:k + 1, :] == expert, 1.0, 0.0)
    before = jnp.where(expert < other, 1.0, 0.0).astype(jnp.bfloat16)
    rank = jnp.dot(chosen.astype(jnp.bfloat16), before, preferred_element_type=jnp.float32)
    rank = jnp.where(chosen > 0.5, rank, -1.0).astype(jnp.bfloat16)
    for out_ref, (first, count) in zip(out_refs, CHUNKS):
        slots = out_ref.shape[0]
        slot = lax.broadcasted_iota(jnp.int32, (slots, tokens), 0)
        column = lax.broadcasted_iota(jnp.int32, (slots, tokens), 1)
        spread = jnp.where(slot // count == column, 1.0, 0.0).astype(jnp.bfloat16)
        ranks = jnp.dot(spread, rank, preferred_element_type=jnp.float32)
        wanted = (slot % count + first).astype(jnp.float32)
        pick = jnp.where(ranks == wanted, 1.0, 0.0).astype(jnp.bfloat16)
        out_ref[...] = jnp.dot(pick, normed, preferred_element_type=jnp.float32).astype(jnp.bfloat16)


def dispatch(routes, expert_input, moe_gain, experts):
    return pl.pallas_call(
        dispatch_kernel,
        out_shape=[
            jax.ShapeDtypeStruct((experts * count, expert_input.shape[1]), jnp.bfloat16) for unused, count in CHUNKS
        ],
        name="dispatch",
    )(routes.T, expert_input, moe_gain.reshape(1, -1))


def combine_kernel(routes_ref, weight_ref, *refs, chunks, carried):
    out_ref = refs[-1]
    tokens = routes_ref.shape[0]
    row = lax.broadcasted_iota(jnp.int32, (tokens, tokens), 0)
    expert = lax.broadcasted_iota(jnp.int32, (tokens, tokens), 1)
    chosen = jnp.zeros((tokens, tokens), jnp.float32)
    scale = jnp.zeros((tokens, tokens), jnp.float32)
    for k in range(routes_ref.shape[1]):
        match = routes_ref[:, k:k + 1] == expert
        chosen = chosen + jnp.where(match, 1.0, 0.0)
        scale = scale + jnp.where(match, weight_ref[:, k:k + 1], 0.0)
    before = jnp.where(expert < row, 1.0, 0.0).astype(jnp.bfloat16)
    rank = jnp.dot(before, chosen.astype(jnp.bfloat16), preferred_element_type=jnp.float32)
    rank = jnp.where(chosen > 0.5, rank, -1.0).astype(jnp.bfloat16)
    high = scale.astype(jnp.bfloat16)
    low = (scale - high.astype(jnp.float32)).astype(jnp.bfloat16)
    total = refs[len(chunks)][...] if carried else None
    for rows_ref, (first, count) in zip(refs, chunks):
        slots = rows_ref.shape[0]
        slot = lax.broadcasted_iota(jnp.int32, (tokens, slots), 1)
        line = lax.broadcasted_iota(jnp.int32, (tokens, slots), 0)
        spread = jnp.where(slot // count == line, 1.0, 0.0).astype(jnp.bfloat16)
        ranks = jnp.dot(rank, spread, preferred_element_type=jnp.float32)
        here = ranks == (slot % count + first).astype(jnp.float32)
        returned = rows_ref[...]
        for part in (high, low):
            picked = jnp.where(here, jnp.dot(part, spread, preferred_element_type=jnp.float32), 0.0)
            piece = jnp.dot(picked.astype(jnp.bfloat16), returned, preferred_element_type=jnp.float32)
            total = piece if total is None else total + piece
    out_ref[...] = total.astype(out_ref.dtype)


def combine(routes, route_weight, returned, chunks, carried, kind):
    arrays = list(returned) + ([] if carried is None else [carried])
    return pl.pallas_call(
        functools.partial(combine_kernel, chunks=chunks, carried=carried is not None),
        out_shape=jax.ShapeDtypeStruct((routes.shape[0], returned[0].shape[1]), kind),
        name="combine",
    )(routes, route_weight, *arrays)


def expert_rows(rows_in, gate_matrix, up_matrix, down_matrix):
    gate_pre = jnp.dot(rows_in, gate_matrix, preferred_element_type=jnp.float32)
    up_pre = jnp.dot(rows_in, up_matrix, preferred_element_type=jnp.float32)
    clipped = jnp.minimum(gate_pre, 7.0)
    up_clip = jnp.clip(up_pre, -7.0, 7.0)
    activated = ((up_clip + 1.0) * clipped * jax.nn.sigmoid(1.702 * clipped)).astype(jnp.bfloat16)
    return jnp.dot(activated, down_matrix, preferred_element_type=jnp.float32).astype(jnp.bfloat16)


def shards(
    queries,
    keys,
    values,
    head_lambda,
    out_gain,
    expert_input,
    routes,
    route_weight,
    moe_gain,
    gate_weight,
    up_weight,
    down_weight,
):
    ep_count = lax.axis_size("ep")
    me = lax.axis_index("ep")
    partner = ep_count - 1 - me
    half = queries.shape[0] // 2
    swap = [(i, ep_count - 1 - i) for i in range(ep_count)]

    outgoing = dispatch(routes, expert_input, moe_gain, ep_count)
    arrived = [lax.all_to_all(rows, "ep", split_axis=0, concat_axis=0, tiled=True) for rows in outgoing]
    gathered = [lax.all_gather(rows, "tp", axis=0, tiled=True) for rows in arrived]

    other_queries = lax.ppermute(queries[half:], "ep", swap)
    both = jnp.concatenate([keys, values], axis=1)
    both = lax.all_gather(both, "ep", axis=0, tiled=True)
    starts = jnp.stack([2 * half * me, 2 * half * partner + half]).astype(jnp.int32)
    mixed = attention(
        starts,
        head_lambda,
        out_gain.reshape(1, -1),
        jnp.stack([queries[:half], other_queries]),
        both[:, :2 * HEAD],
        both[:, 2 * HEAD:],
    )
    mixed_out = jnp.concatenate([mixed[0], lax.ppermute(mixed[1], "ep", swap)], axis=0)

    partial = [expert_rows(rows, gate_weight[0], up_weight[0], down_weight[0]) for rows in gathered]
    summed = [lax.psum_scatter(rows, "tp", scatter_dimension=0, tiled=True) for rows in partial]
    returned = [lax.all_to_all(rows, "ep", split_axis=0, concat_axis=0, tiled=True) for rows in summed]
    early = combine(routes, route_weight, returned[1:], CHUNKS[1:], None, jnp.float32)
    expert_mix = combine(routes, route_weight, returned[:1], CHUNKS[:1], early, jnp.bfloat16)
    return (mixed_out, expert_mix)


def solution(mesh):
    placed = (
        P("ep", "tp"),
        P("ep", "tp"),
        P("ep", "tp"),
        P("tp"),
        P(),
        P(("ep", "tp"), None),
        P(("ep", "tp"), None),
        P(("ep", "tp"), None),
        P(),
        P("ep", None, "tp"),
        P("ep", None, "tp"),
        P("ep", "tp", None),
    )
    return jax.shard_map(
        shards,
        mesh=mesh,
        in_specs=placed,
        out_specs=(P("ep", "tp"), P(("ep", "tp"), None)),
        check_vma=False,
    )
```

time: 553 us -> 421 us (0.76)
  matrix products: 158 us -> 43.7 us
  other arithmetic: 52.5 us -> 1.55 us
  Pallas kernels: 0 us -> 45.9 us
  local copies, waits for them, and re-layouts: 54.4 us -> 16.5 us
  loops' own time: 21.2 us -> 0 us
  starting transfers between devices: 8.05 us -> 24.1 us
  waiting for transfers between devices: 197 us -> 213 us
  blocking collectives: 44 us -> 58.6 us
    dot_general x66 -> x6, matrix products: 158 us -> 43.7 us  [the longest x3 26.7 us: expert_rows(): jnp.dot(activated, down_matrix, preferred_element_type=jnp.float32)]
    pallas_call x0 -> x4, Pallas kernels: none -> 45.9 us  [the longest x1 35.5 us: attention(): pl.pallas_call(attention_kernel, grid=(groups,), in_specs=[pl.BlockSpec(m...]
    reduce_sum x36 -> x0, other arithmetic: 37.4 us -> none  [the longest x32 29.6 us: update(): new_total = factor * run_total + jnp.sum(weights, axis=-1)]
    another operation x33 -> x0, loops' own time: 21.2 us -> none  [the longest x1 19 us: shards(): folded = lax.fori_loop(0, piece_rows // block_len, block_step, initial)]
    gather x3 -> x0, local copies, waits for them, and re-layouts: 16.8 us -> none  [the longest x2 9.27 us: shards(): normed[slot_token]]
    all_to_all x1 -> x3, starting transfers between devices: 7.75 us -> 23.1 us  [shards(): lax.all_to_all(rows, 'ep', split_axis=0, concat_axis=0, tiled=True)]
    ppermute x0 -> x2, waiting for transfers between devices: none -> 15.1 us  [the longest x1 9.98 us: shards(): other_queries = lax.ppermute(queries[half:], 'ep', swap)]
    all_to_all x1 -> x3, blocking collectives: 44 us -> 58.6 us  [shards(): lax.all_to_all(rows, 'ep', split_axis=0, concat_axis=0, tiled=True)]
  transfers between devices with their start and end apart: 4 -> 12, of which waited for: 2 -> 8; matrix products, arithmetic and copies ran while one was open for 32% -> 13% of each run, Pallas kernels for 0% -> 8%
where the time goes in v1:
time: 421 us; the launch traced here: 418 us
  waiting for transfers between devices  213 us (51%)
  blocking collectives  58.6 us (14%)
  Pallas kernels  45.9 us (11%)
  matrix products  43.7 us (10%)
  starting transfers between devices  24.1 us (6%)
  local copies, waits for them, and re-layouts  16.5 us (4%)
  between operations  14.3 us (3%)
    reduce_scatter x3, waiting for transfers between devices, shards(): lax.psum_scatter(rows, 'tp', scatter_dimension=0, tiled=True)  88.9 us
    all_gather x3, waiting for transfers between devices, shards(): lax.all_gather(rows, 'tp', axis=0, tiled=True)  59.3 us
    all_to_all x3, blocking collectives, shards(): lax.all_to_all(rows, 'ep', split_axis=0, concat_axis=0, tiled=True)  58.6 us
    all_gather x1, waiting for transfers between devices, shards(): both = lax.all_gather(both, 'ep', axis=0, tiled=True)  49.9 us
    pallas_call x1, Pallas kernels, attention(): pl.pallas_call(attention_kernel, grid=(groups,), in_specs=[pl.BlockSpec(m...  35.5 us
    dot_general x3, matrix products, expert_rows(): jnp.dot(activated, down_matrix, preferred_element_type=jnp.float32)  26.7 us
    all_to_all x3, starting transfers between devices, shards(): lax.all_to_all(rows, 'ep', split_axis=0, concat_axis=0, tiled=True)  23.1 us
    dot_general x2, matrix products, expert_rows(): up_pre = jnp.dot(rows_in, up_matrix, preferred_element_type=jnp.float32)  13.2 us
  transfers between devices with their start and end apart: 12, of which 8 were waited for; matrix products, arithmetic and copies ran while one was open for 13% of the time, Pallas kernels for 8%

profile of v1, /device:TPU:121, one launch (start us, length us, event | category | flops | bytes accessed | tf_op | source)
XLA Modules:
  0.0 418.0 jit_solution(13254975058797980250)
XLA Ops:
  7.2 0.0 all-gather.7.cloned.1.call-start
  7.2 3.5 dispatch.1
  10.7 1.2 all_to_all.45
  11.9 15.8 %all_to_all.69 = bf16[32,4,2048]{2,1,0:T(4,128)(2,1)S(1)} all-to-all(bf16[32,4,2048]{2,1,0:T(4,128)(2,1)S(1)} %all_to_all.45), channel_id=1, replica_groups=mesh['ep'=32,'tp'=4] {'ep'}, dimensions={0} | all-to-all | bytes 1048576 | tf_op jit(solution)/shard_map/all_to_all | solution.py:198
  27.7 0.9 all_to_all.47
  28.6 0.0 all-gather.11.cloned.1.call-start
  28.7 21.9 %all_to_all.70 = bf16[32,8,2048]{2,1,0:T(8,128)(2,1)} all-to-all(bf16[32,8,2048]{2,1,0:T(8,128)(2,1)} %bitcast.76), channel_id=1, replica_groups=mesh['ep'=32,'tp'=4] {'ep'}, dimensions={0} | all-to-all | bytes 2097152 | tf_op jit(solution)/shard_map/all_to_all | solution.py:198
  50.6 0.0 all-gather.11.cloned.1.call-update
  50.7 0.0 all-gather.9.cloned.1.call-start
  50.7 20.9 %all_to_all.71 = bf16[32,8,2048]{2,1,0:T(8,128)(2,1)} all-to-all(bf16[32,8,2048]{2,1,0:T(8,128)(2,1)S(1)} %bitcast.75), channel_id=1, replica_groups=mesh['ep'=32,'tp'=4] {'ep'}, dimensions={0} | all-to-all | bytes 2097152 | tf_op jit(solution)/shard_map/all_to_all | solution.py:198
  71.6 0.0 reduce-scatter.4.cloned.1.call-start
  71.7 0.0 all-gather.7.cloned.1.call-done
  71.7 3.8 fusion.22
  75.5 6.1 %convolution_convert_fusion.2 = bf16[512,2048]{1,0:T(8,128)(2,1)} fusion(bf16[1,512,2048]{2,1,0:T(8,128)(2,1)S(1)} %copy-done, f32[512,512]{1,0:T(8,128)S(1)} %fusion.22, bf16[512,2048]{1,0:T(8,128)(2,1)} %all-gather.7.cloned.1.call-done, bf16[1,2048,512]{2,1,0:T(8,128)(2,1)} %param.22), kind=kOutput, calls=%fused_computation.2 | convolution fusion | flops 2150891520 | bytes 9437184 | tf_op jit(solution)/shard_map/dot_general | solution.py:174
  81.6 0.0 reduce-scatter.8.cloned.1.call-start
  81.7 27.9 %all-gather.11.cloned.1.call-done = bf16[1024,2048]{1,0:T(8,128)(2,1)} async-done(((bf16[256,2048]{1,0:T(8,128)(2,1)}), bf16[1024,2048]{1,0:T(8,128)(2,1)}) %all-gather.11.cloned.1.call-update) | async-done | bytes 4194320 | tf_op jit(solution)/shard_map/all_gather | solution.py:199
  109.6 6.6 %fusion.9 = f32[1024,512]{1,0:T(8,128)} fusion(bf16[1024,2048]{1,0:T(8,128)(2,1)} %all-gather.11.cloned.1.call-done, bf16[1,2048,512]{2,1,0:T(8,128)(2,1)} %param.22), kind=kOutput, calls=%fused_computation.12 | convolution fusion | flops 2147483648 | bytes 8388608 | tf_op jit(solution)/shard_map/dot_general | solution.py:170
  116.2 10.3 %convolution_convert_fusion = bf16[1024,2048]{1,0:T(8,128)(2,1)} fusion(bf16[1,512,2048]{2,1,0:T(8,128)(2,1)S(1)} %copy-done, f32[1024,512]{1,0:T(8,128)} %fusion.9, bf16[1024,2048]{1,0:T(8,128)(2,1)} %all-gather.11.cloned.1.call-done, bf16[1,2048,512]{2,1,0:T(8,128)(2,1)} %param.21), kind=kOutput, calls=%fused_computation | convolution fusion | flops 4302307328 | bytes 14680064 | tf_op jit(solution)/shard_map/dot_general | solution.py:174
  126.5 0.0 all-gather.5.cloned.1.call-start
  126.6 0.8 copy-done.8
  127.4 0.1 copy-done.9
  127.5 0.7 pad_maximum_fusion.1
  128.2 0.2 reduce-scatter.6.cloned.1.call-start
  128.5 31.4 %all-gather.9.cloned.1.call-done = bf16[1024,2048]{1,0:T(8,128)(2,1)} async-done(((bf16[256,2048]{1,0:T(8,128)(2,1)}), bf16[1024,2048]{1,0:T(8,128)(2,1)}) %all-gather.9.cloned.1.call-update) | async-done | bytes 4194320 | tf_op jit(solution)/shard_map/all_gather | solution.py:199
  159.8 6.6 %fusion.11 = f32[1024,512]{1,0:T(8,128)} fusion(bf16[1024,2048]{1,0:T(8,128)(2,1)} %all-gather.9.cloned.1.call-done, bf16[1,2048,512]{2,1,0:T(8,128)(2,1)} %param.22), kind=kOutput, calls=%fused_computation.14 | convolution fusion | flops 2147483648 | bytes 8388608 | tf_op jit(solution)/shard_map/dot_general | solution.py:170
  166.4 10.3 %convolution_convert_fusion.1 = bf16[1024,2048]{1,0:T(8,128)(2,1)} fusion(bf16[1,512,2048]{2,1,0:T(8,128)(2,1)S(1)} %copy-done, f32[1024,512]{1,0:T(8,128)} %fusion.11, bf16[1024,2048]{1,0:T(8,128)(2,1)} %all-gather.9.cloned.1.call-done, bf16[1,2048,512]{2,1,0:T(8,128)(2,1)} %param.21), kind=kOutput, calls=%fused_computation.1 | convolution fusion | flops 4302307328 | bytes 14680064 | tf_op jit(solution)/shard_map/dot_general | solution.py:174
  176.7 15.5 %reduce-scatter.4.cloned.1.call-done = bf16[128,2048]{1,0:T(8,128)(2,1)} async-done(((bf16[512,2048]{1,0:T(8,128)(2,1)}), bf16[128,2048]{1,0:T(8,128)(2,1)}) %reduce-scatter.4.cloned.1.call-update) | async-done | bytes 524304 | tf_op jit(solution)/shard_map/reduce_scatter | solution.py:216
  192.2 2.0 all_to_all.48
  194.2 7.7 %all-to-all-start.1 = ((bf16[32,4,2048]{2,1,0:T(4,128)(2,1)}), bf16[32,4,2048]{2,1,0:T(4,128)(2,1)S(1)}, u32[]{:S(2)}, u32[]{:S(2)}) async-start(bf16[32,4,2048]{2,1,0:T(4,128)(2,1)} %all_to_all.48), calls=%async_computation.2 | async-start | bytes 1048576 | tf_op jit(solution)/shard_map/all_to_all | solution.py:217
  202.0 0.2 collective-permute-start
  202.2 0.1 pad_add_fusion.start_ref
  202.3 10.0 %collective-permute-done = bf16[256,256]{1,0:T(8,128)(2,1)S(1)} collective-permute-done((bf16[256,256]{1,0:T(8,128)(2,1)S(1)}, bf16[256,256]{1,0:T(8,128)(2,1)S(1)}, u32[]{:S(2)}, u32[]{:S(2)}) %collective-permute-start) | collective-permute-done | bytes 131104 | tf_op jit(solution)/shard_map/ppermute | solution.py:201
  212.3 28.7 %reduce-scatter.8.cloned.1.call-done = bf16[256,2048]{1,0:T(8,128)(2,1)} async-done(((bf16[1024,2048]{1,0:T(8,128)(2,1)}), bf16[256,2048]{1,0:T(8,128)(2,1)}) %reduce-scatter.8.cloned.1.call-update) | async-done | bytes 1048592 | tf_op jit(solution)/shard_map/reduce_scatter | solution.py:216
  241.1 7.7 %all-to-all-start.5 = ((bf16[32,8,2048]{2,1,0:T(8,128)(2,1)}), bf16[32,8,2048]{2,1,0:T(8,128)(2,1)S(1)}, u32[]{:S(2)}, u32[]{:S(2)}) async-start(bf16[32,8,2048]{2,1,0:T(8,128)(2,1)} %bitcast.74), calls=%async_computation.8 | async-start | bytes 2097152 | tf_op jit(solution)/shard_map/all_to_all | solution.py:217
  248.7 49.9 %all-gather.5.cloned.1.call-done = bf16[16384,256]{1,0:T(8,128)(2,1)} async-done(((bf16[512,256]{1,0:T(8,128)(2,1)}), bf16[16384,256]{1,0:T(8,128)(2,1)}) %all-gather.5.cloned.1.call-update) | async-done | bytes 8388624 | tf_op jit(solution)/shard_map/all_gather | solution.py:203
  298.7 5.7 %fusion.59 = (bf16[16384,128]{1,0:T(8,128)(2,1)}, bf16[16384,128]{1,0:T(8,128)(2,1)}) fusion(bf16[16384,256]{1,0:T(8,128)(2,1)} %all-gather.5.cloned.1.call-done), kind=kLoop, calls=%fused_computation.49 | loop fusion | bytes 16777216 | tf_op jit(solution)/shard_map/slice | solution.py:211
  304.4 44.7 %reduce-scatter.6.cloned.1.call-done = bf16[256,2048]{1,0:T(8,128)(2,1)} async-done(((bf16[1024,2048]{1,0:T(8,128)(2,1)}), bf16[256,2048]{1,0:T(8,128)(2,1)}) %reduce-scatter.6.cloned.1.call-update) | async-done | bytes 1048592 | tf_op jit(solution)/shard_map/reduce_scatter | solution.py:216
  349.1 7.7 %all-to-all-start.3 = ((bf16[32,8,2048]{2,1,0:T(8,128)(2,1)}), bf16[32,8,2048]{2,1,0:T(8,128)(2,1)}, u32[]{:S(2)}, u32[]{:S(2)}) async-start(bf16[32,8,2048]{2,1,0:T(8,128)(2,1)} %bitcast.73), calls=%async_computation.5 | async-start | bytes 2097152 | tf_op jit(solution)/shard_map/all_to_all | solution.py:217
  356.9 2.2 copy-done.1
  359.1 35.5 %attention.1 = bf16[2,256,256]{2,1,0:T(8,128)(2,1)S(1)} custom-call(s32[2]{0:T(128)S(1)} %pad_add_fusion.start_ref, f32[2]{0:T(128)S(1)} %copy-done.2, f32[1,128]{1,0:T(1,128)S(1)} %bitcast.69, bf16[2,256,256]{2,1,0:T(8,128)(2,1)S(1)} %pad_maximum_fusion.query_ref, bf16[16384,128]{1,0:T(8,128)(2,1)S(1)} %copy-done.1, ...), custom_call_target="tpu_custom_call" | custom-call | flops 17999998976 | bytes 9000000 | tf_op jit(solution)/shard_map/attention/pallas_call | solution.py:70
  394.6 0.3 collective-permute-start.1
  394.9 0.7 copy.16.routes_ref
  395.7 0.7 copy.17.weight_ref
  396.4 2.0 all_to_all.50.refs_0_
  398.4 5.1 %collective-permute-done.1 = bf16[256,256]{1,0:T(8,128)(2,1)S(1)} collective-permute-done((bf16[256,256]{1,0:T(8,128)(2,1)S(1)}, bf16[256,256]{1,0:T(8,128)(2,1)S(1)}, u32[]{:S(2)}, u32[]{:S(2)}) %collective-permute-start.1) | collective-permute-done | bytes 131104 | tf_op jit(solution)/shard_map/ppermute | solution.py:213
  403.5 0.7 pad_maximum_fusion.2
  404.2 3.7 combine.2.refs_1_
  408.0 3.2 combine.3
  (33 shorter events, 0.2 us)
Async XLA Ops:
  7.2 68.3 %copy-start = (bf16[1,512,2048]{2,1,0:T(8,128)(2,1)S(1)}, bf16[1,512,2048]{2,1,0:T(8,128)(2,1)}, u32[]{:S(2)}) copy-start(bf16[1,512,2048]{2,1,0:T(8,128)(2,1)} %param.23) | copy-start | bytes 6291460
  7.2 64.5 %all-gather.7.cloned.1.call-start = ((), (), s32[]{:S(2)}) async-start(), calls=%async_computation.10 | async-start | bytes 2621440 | tf_op jit(solution)/shard_map/all_gather | solution.py:199
  28.6 22.1 %copy-start.6 = (bf16[256,2048]{1,0:T(8,128)(2,1)S(1)}, bf16[256,2048]{1,0:T(8,128)(2,1)}, u32[]{:S(2)}) copy-start(bf16[256,2048]{1,0:T(8,128)(2,1)} %get-tuple-element.6) | copy-start | bytes 3145732
  28.6 80.9 %all-gather.11.cloned.1.call-start = ((), (), s32[]{:S(2)}) async-start(), calls=%async_computation.14 | async-start | bytes 5242880 | tf_op jit(solution)/shard_map/all_gather | solution.py:199
  50.7 109.2 %all-gather.9.cloned.1.call-start = ((), (), s32[]{:S(2)}) async-start(), calls=%async_computation.12 | async-start | bytes 5242880 | tf_op jit(solution)/shard_map/all_gather | solution.py:199
  71.6 120.6 %reduce-scatter.4.cloned.1.call-start = ((), (), s32[]{:S(2)}) async-start(), calls=%async_computation.11 | async-start | bytes 2621440 | tf_op jit(solution)/shard_map/reduce_scatter | solution.py:216
  81.6 159.5 %reduce-scatter.8.cloned.1.call-start = ((), (), s32[]{:S(2)}) async-start(), calls=%async_computation.15 | async-start | bytes 5242880 | tf_op jit(solution)/shard_map/reduce_scatter | solution.py:216
  126.5 0.9 copy-start.8
  126.5 1.0 copy-start.9
  126.5 172.1 %all-gather.5.cloned.1.call-start = ((), (), s32[]{:S(2)}) async-start(), calls=%async_computation.9 | async-start | bytes 8650752 | tf_op jit(solution)/shard_map/all_gather | solution.py:203
  128.2 220.9 %reduce-scatter.6.cloned.1.call-start = ((), (), s32[]{:S(2)}) async-start(), calls=%async_computation.13 | async-start | bytes 5242880 | tf_op jit(solution)/shard_map/reduce_scatter | solution.py:216
  176.7 25.2 %copy-start.7 = (bf16[512,256]{1,0:T(8,128)(2,1)S(1)}, bf16[512,256]{1,0:T(8,128)(2,1)}, u32[]{:S(2)}) copy-start(bf16[512,256]{1,0:T(8,128)(2,1)} %param.12) | copy-start | bytes 786436
  194.2 18.1 %all-to-all-start.1 = ((bf16[32,4,2048]{2,1,0:T(4,128)(2,1)}), bf16[32,4,2048]{2,1,0:T(4,128)(2,1)S(1)}, u32[]{:S(2)}, u32[]{:S(2)}) async-start(bf16[32,4,2048]{2,1,0:T(4,128)(2,1)} %all_to_all.48), calls=%async_computation.2 | async-start | bytes 1048576 | tf_op jit(solution)/shard_map/all_to_all | solution.py:217
  202.0 10.3 %collective-permute-start = (bf16[256,256]{1,0:T(8,128)(2,1)S(1)}, bf16[256,256]{1,0:T(8,128)(2,1)S(1)}, u32[]{:S(2)}, u32[]{:S(2)}) collective-permute-start(bf16[256,256]{1,0:T(8,128)(2,1)S(1)} %get-tuple-element.13), channel_id=1, source_target_pairs={{0,124},{4,120},{8,116},{12,112},{16,108},{20,104},{24,100},{28,96... | collective-permute-start | bytes 393224 | tf_op jit(solution)/shard_map/ppermute | solution.py:201
  212.3 28.8 %copy-start.5 = (bf16[32,4,2048]{2,1,0:T(4,128)(2,1)}, bf16[32,4,2048]{2,1,0:T(4,128)(2,1)S(1)}, u32[]{:S(2)}) copy-start(bf16[32,4,2048]{2,1,0:T(4,128)(2,1)S(1)} %all-to-all-done.1) | copy-start | bytes 1572868
  241.1 108.1 %all-to-all-start.5 = ((bf16[32,8,2048]{2,1,0:T(8,128)(2,1)}), bf16[32,8,2048]{2,1,0:T(8,128)(2,1)S(1)}, u32[]{:S(2)}, u32[]{:S(2)}) async-start(bf16[32,8,2048]{2,1,0:T(8,128)(2,1)} %bitcast.74), calls=%async_computation.8 | async-start | bytes 2097152 | tf_op jit(solution)/shard_map/all_to_all | solution.py:217
  304.4 52.4 %copy-start.2 = (f32[2]{0:T(128)S(1)}, f32[2]{0:T(128)}, u32[]{:S(2)}) copy-start(f32[2]{0:T(128)} %lambda_ref.1) | copy-start | bytes 28
  304.4 52.5 %copy-start.3 = (f32[128]{0:T(128)S(1)}, f32[128]{0:T(128)}, u32[]{:S(2)}) copy-start(f32[128]{0:T(128)} %param.16) | copy-start | bytes 1540
  349.1 45.5 %copy-start.4 = (bf16[32,8,2048]{2,1,0:T(8,128)(2,1)}, bf16[32,8,2048]{2,1,0:T(8,128)(2,1)S(1)}, u32[]{:S(2)}) copy-start(bf16[32,8,2048]{2,1,0:T(8,128)(2,1)S(1)} %all-to-all-done.5) | copy-start | bytes 3145732
  349.1 55.1 %all-to-all-start.3 = ((bf16[32,8,2048]{2,1,0:T(8,128)(2,1)}), bf16[32,8,2048]{2,1,0:T(8,128)(2,1)}, u32[]{:S(2)}, u32[]{:S(2)}) async-start(bf16[32,8,2048]{2,1,0:T(8,128)(2,1)} %bitcast.73), calls=%async_computation.5 | async-start | bytes 2097152 | tf_op jit(solution)/shard_map/all_to_all | solution.py:217
  356.9 2.2 copy-start.1
  359.1 35.8 %copy-start.10 = (s32[128,4]{0,1:T(4,128)S(1)}, s32[128,4]{0,1:T(4,128)}, u32[]{:S(2)}) copy-start(s32[128,4]{0,1:T(4,128)} %param.18) | copy-start | bytes 6148
  359.1 36.6 %copy-start.11 = (f32[128,4]{0,1:T(4,128)S(1)}, f32[128,4]{0,1:T(4,128)}, u32[]{:S(2)}) copy-start(f32[128,4]{0,1:T(4,128)} %param.19) | copy-start | bytes 6148
  394.6 8.9 %collective-permute-start.1 = (bf16[256,256]{1,0:T(8,128)(2,1)S(1)}, bf16[256,256]{1,0:T(8,128)(2,1)S(1)}, u32[]{:S(2)}, u32[]{:S(2)}) collective-permute-start(bf16[256,256]{1,0:T(8,128)(2,1)S(1)} %get-tuple-element.11), channel_id=1, source_target_pairs={{0,124},{4,120},{8,116},{12,112},{16,108},{20,104},{24,100},{28,96... | collective-permute-start | bytes 393224 | tf_op jit(solution)/shard_map/ppermute | solution.py:213
Sparse Core Ops, SparseCore 0:
  28.8 30.8 all-gather.6
  61.4 48.1 all-gather.10
  111.3 48.5 all-gather.8
  162.1 30.0 reduce-scatter.3
  194.5 46.5 reduce-scatter.7
  243.8 54.8 all-gather.4
  301.1 48.0 reduce-scatter.5

commit v2 on v1

--- a/solution.py
+++ b/solution.py
@@ -7,20 +7,19 @@
 from jax.experimental.pallas import tpu as pltpu
 from jax.sharding import PartitionSpec as P
 
-HEADS = 8
-KV_HEADS = 4
+
 HEAD = 64
 VDIM = 128
 LOG2E = 1.4426950408889634
 KEY_BLOCK = 1024
-CHUNKS = ((0, 4), (4, 8), (12, 8))
+CHUNKS = ((0, 8), (8, 8), (16, 4))
+FAR_STEP = (1, -1, -1)
 
 epsilon = 1e-05
 
 
-def attention_kernel(start_ref, lambda_ref, gain_ref, query_ref, key_ref, value_ref, out_ref, max_ref, sum_ref):
-    group = pl.program_id(0)
-    start = start_ref[group]
+def attention_kernel(start_ref, lambda_ref, gain_ref, query_ref, key_value_ref, out_ref, max_ref, sum_ref):
+    start = start_ref[pl.program_id(0)]
     rows = query_ref.shape[1]
     lane = lax.broadcasted_iota(jnp.int32, (rows, 2 * HEAD), 1)
     max_ref[...] = jnp.full(max_ref.shape, -1e30, jnp.float32)
@@ -28,8 +27,8 @@
     ones = jnp.ones((KEY_BLOCK, VDIM), jnp.bfloat16)
 
     def one_block(offset, masked):
-        keys = key_ref[pl.ds(offset, KEY_BLOCK), :]
-        values = jnp.concatenate([value_ref[pl.ds(offset, KEY_BLOCK), :], ones], axis=1)
+        keys = key_value_ref[pl.ds(offset, KEY_BLOCK), :2 * HEAD]
+        values = jnp.concatenate([key_value_ref[pl.ds(offset, KEY_BLOCK), 2 * HEAD:], ones], axis=1)
         if masked:
             column = lax.broadcasted_iota(jnp.int32, (rows, KEY_BLOCK), 1) + offset
             row = lax.broadcasted_iota(jnp.int32, (rows, KEY_BLOCK), 0) + start
@@ -64,9 +63,9 @@
         out_ref[0, :, head * VDIM:(head + 1) * VDIM] = (combined * inverse * gain_ref[...]).astype(jnp.bfloat16)
 
 
-def attention(starts, head_lambda, out_gain, query_sets, keys, values):
+def attention(starts, head_lambda, out_gain, query_sets, keys_values):
     groups, rows, width = query_sets.shape
-    length = keys.shape[0]
+    length, both = keys_values.shape
     return pl.pallas_call(
         attention_kernel,
         grid=(groups,),
@@ -75,8 +74,7 @@
             pl.BlockSpec(memory_space=pltpu.SMEM),
             pl.BlockSpec((1, VDIM), lambda g: (0, 0)),
             pl.BlockSpec((1, rows, width), lambda g: (g, 0, 0)),
-            pl.BlockSpec((length, 2 * HEAD), lambda g: (0, 0)),
-            pl.BlockSpec((length, VDIM), lambda g: (0, 0)),
+            pl.BlockSpec((length, both), lambda g: (0, 0)),
         ],
         out_specs=pl.BlockSpec((1, rows, width), lambda g: (g, 0, 0)),
         out_shape=jax.ShapeDtypeStruct((groups, rows, width), jnp.bfloat16),
@@ -84,10 +82,10 @@
             pltpu.VMEM((4, rows, 1), jnp.float32),
             pltpu.VMEM((4, rows, 2 * VDIM), jnp.float32),
         ],
-        compiler_params=pltpu.CompilerParams(vmem_limit_bytes=48 * 1024 * 1024),
+        compiler_params=pltpu.CompilerParams(vmem_limit_bytes=60 * 1024 * 1024),
         cost_estimate=pl.CostEstimate(flops=18_000_000_000, transcendentals=18_000_000, bytes_accessed=9_000_000),
         name="attention",
-    )(starts, head_lambda, out_gain, query_sets, keys, values)
+    )(starts, head_lambda, out_gain, query_sets, keys_values)
 
 
 def dispatch_kernel(routes_ref, input_ref, gain_ref, *out_refs):
@@ -165,16 +163,105 @@
     )(routes, route_weight, *arrays)
 
 
-def expert_rows(rows_in, gate_matrix, up_matrix, down_matrix):
-    gate_pre = jnp.dot(rows_in, gate_matrix, preferred_element_type=jnp.float32)
-    up_pre = jnp.dot(rows_in, up_matrix, preferred_element_type=jnp.float32)
-    clipped = jnp.minimum(gate_pre, 7.0)
-    up_clip = jnp.clip(up_pre, -7.0, 7.0)
-    activated = ((up_clip + 1.0) * clipped * jax.nn.sigmoid(1.702 * clipped)).astype(jnp.bfloat16)
-    return jnp.dot(activated, down_matrix, preferred_element_type=jnp.float32).astype(jnp.bfloat16)
-
-
-def shards(
+def expert_kernel(gate_hbm, up_hbm, down_hbm, *refs, sizes, addends):
+    count, extra = len(sizes), sum(addends)
+    row_hbm, extra_hbm, out_hbm = refs[:count], refs[count:count + extra], refs[count + extra:2 * count + extra]
+    gate_ref, up_ref, down_ref, row_ref, out_ref, gate_sem, up_sem, down_sem, row_sem, out_sem = refs[2 * count + extra:][:10]
+    extra_refs = refs[2 * count + extra + 10:]
+    extra_loads = [
+        pltpu.make_async_copy(extra_hbm[i], extra_refs[i], extra_refs[extra].at[i]) for i in range(extra)
+    ]
+    begins = [sum(sizes[:i]) for i in range(count)]
+    loads = [
+        pltpu.make_async_copy(row_hbm[i], row_ref.at[pl.ds(begins[i], sizes[i]), :], row_sem.at[i]) for i in range(count)
+    ]
+    gate_load = pltpu.make_async_copy(gate_hbm, gate_ref, gate_sem)
+    up_load = pltpu.make_async_copy(up_hbm, up_ref, up_sem)
+    down_load = pltpu.make_async_copy(down_hbm, down_ref, down_sem)
+    loads[0].start()
+    gate_load.start()
+    up_load.start()
+    down_load.start()
+    for load in loads[1:]:
+        load.start()
+    for load in extra_loads:
+        load.start()
+    stores = []
+    used = 0
+    for i in range(count):
+        loads[i].wait()
+        rows = row_ref[pl.ds(begins[i], sizes[i]), :]
+        if i == 0:
+            gate_load.wait()
+        gate_pre = jnp.dot(rows, gate_ref[...], preferred_element_type=jnp.float32)
+        if i == 0:
+            up_load.wait()
+        up_pre = jnp.dot(rows, up_ref[...], preferred_element_type=jnp.float32)
+        clipped = jnp.minimum(gate_pre, 7.0)
+        up_clip = jnp.clip(up_pre, -7.0, 7.0)
+        activated = ((up_clip + 1.0) * clipped * jax.nn.sigmoid(1.702 * clipped)).astype(jnp.bfloat16)
+        if i == 0:
+            down_load.wait()
+        partial = jnp.dot(activated, down_ref[...], preferred_element_type=jnp.float32)
+        for j in range(used, used + addends[i]):
+            extra_loads[j].wait()
+            partial = partial + extra_refs[j][...].astype(jnp.float32)
+        used += addends[i]
+        out_ref[pl.ds(begins[i], sizes[i]), :] = partial.astype(jnp.bfloat16)
+        store = pltpu.make_async_copy(out_ref.at[pl.ds(begins[i], sizes[i]), :], out_hbm[i], out_sem.at[i])
+        store.start()
+        stores.append(store)
+    for store in stores:
+        store.wait()
+
+
+def expert(rows, weights, addends):
+    width, hidden = weights[0].shape
+    sizes = tuple(r.shape[0] for r in rows)
+    total = sum(sizes)
+    extra = [a for more in addends for a in more]
+    return pl.pallas_call(
+        functools.partial(expert_kernel, sizes=sizes, addends=tuple(len(more) for more in addends)),
+        in_specs=[pl.BlockSpec(memory_space=pltpu.HBM)] * (3 + len(rows) + len(extra)),
+        out_specs=[pl.BlockSpec(memory_space=pltpu.HBM)] * len(rows),
+        out_shape=[jax.ShapeDtypeStruct(r.shape, jnp.bfloat16) for r in rows],
+        scratch_shapes=[
+            pltpu.VMEM((width, hidden), jnp.bfloat16),
+            pltpu.VMEM((width, hidden), jnp.bfloat16),
+            pltpu.VMEM((hidden, width), jnp.bfloat16),
+            pltpu.VMEM((total, width), jnp.bfloat16),
+            pltpu.VMEM((total, width), jnp.bfloat16),
+            pltpu.SemaphoreType.DMA,
+            pltpu.SemaphoreType.DMA,
+            pltpu.SemaphoreType.DMA,
+            pltpu.SemaphoreType.DMA((len(rows),)),
+            pltpu.SemaphoreType.DMA((len(rows),)),
+        ]
+        + [pltpu.VMEM(a.shape, jnp.bfloat16) for a in extra]
+        + ([pltpu.SemaphoreType.DMA((len(extra),))] if extra else []),
+        compiler_params=pltpu.CompilerParams(vmem_limit_bytes=60 * 1024 * 1024),
+        cost_estimate=pl.CostEstimate(
+            flops=6 * total * width * hidden, transcendentals=total * hidden, bytes_accessed=6 * width * hidden
+        ),
+        name="expert",
+    )(*weights, *rows, *extra)
+
+
+def send(value, step):
+    size = lax.axis_size("tp")
+    return lax.ppermute(value, "tp", [(i, (i + step) % size) for i in range(size)])
+
+
+def swap_ends(value):
+    size = lax.axis_size("ep")
+    return lax.ppermute(value, "ep", [(i, size - 1 - i) for i in range(size)])
+
+
+def exchange(value):
+    return lax.all_to_all(value, "ep", split_axis=0, concat_axis=0, tiled=True)
+
+
+def body(
     queries,
     keys,
     values,
@@ -192,31 +279,43 @@
     me = lax.axis_index("ep")
     partner = ep_count - 1 - me
     half = queries.shape[0] // 2
-    swap = [(i, ep_count - 1 - i) for i in range(ep_count)]
-
+
+    weights = tuple(
+        pltpu.with_memory_space_constraint(w[0], pltpu.HBM) for w in (gate_weight, up_weight, down_weight)
+    )
+
+    other_queries = swap_ends(queries[half:])
     outgoing = dispatch(routes, expert_input, moe_gain, ep_count)
-    arrived = [lax.all_to_all(rows, "ep", split_axis=0, concat_axis=0, tiled=True) for rows in outgoing]
-    gathered = [lax.all_gather(rows, "tp", axis=0, tiled=True) for rows in arrived]
-
-    other_queries = lax.ppermute(queries[half:], "ep", swap)
-    both = jnp.concatenate([keys, values], axis=1)
-    both = lax.all_gather(both, "ep", axis=0, tiled=True)
+
+    gathered = []
+    for name, rows, way in zip("abc", outgoing, FAR_STEP):
+        mine = exchange(rows)
+        if name == "b":
+            keys, values, mine = lax.optimization_barrier((keys, values, mine))
+            both = jnp.concatenate([keys, values], axis=1)
+            both = lax.all_gather(both, "ep", axis=0, tiled=True)
+        behind = send(mine, way)
+        ahead = send(mine, -way)
+        far = send(behind, way)
+        gathered.append((mine, behind, ahead, far))
+
     starts = jnp.stack([2 * half * me, 2 * half * partner + half]).astype(jnp.int32)
-    mixed = attention(
-        starts,
-        head_lambda,
-        out_gain.reshape(1, -1),
-        jnp.stack([queries[:half], other_queries]),
-        both[:, :2 * HEAD],
-        both[:, 2 * HEAD:],
-    )
-    mixed_out = jnp.concatenate([mixed[0], lax.ppermute(mixed[1], "ep", swap)], axis=0)
-
-    partial = [expert_rows(rows, gate_weight[0], up_weight[0], down_weight[0]) for rows in gathered]
-    summed = [lax.psum_scatter(rows, "tp", scatter_dimension=0, tiled=True) for rows in partial]
-    returned = [lax.all_to_all(rows, "ep", split_axis=0, concat_axis=0, tiled=True) for rows in summed]
-    early = combine(routes, route_weight, returned[1:], CHUNKS[1:], None, jnp.float32)
-    expert_mix = combine(routes, route_weight, returned[:1], CHUNKS[:1], early, jnp.bfloat16)
+    query_sets = jnp.stack([queries[:half], other_queries])
+    mixed = attention(starts, head_lambda, out_gain.reshape(1, -1), query_sets, both)
+    mixed_out = jnp.concatenate([mixed[0], swap_ends(mixed[1])], axis=0)
+
+    returned = []
+    for (mine, behind, ahead, far), way in zip(gathered, FAR_STEP):
+        for_far, for_behind = expert([far, behind], weights, [[], []])
+        passing = send(for_far, way)
+        from_ahead = send(for_behind, -way)
+        (for_ahead,) = expert([ahead], weights, [[passing]])
+        from_behind = send(for_ahead, way)
+        (own,) = expert([mine], weights, [[from_ahead, from_behind]])
+        returned.append(exchange(own))
+
+    early = combine(routes, route_weight, returned[:2], CHUNKS[:2], None, jnp.float32)
+    expert_mix = combine(routes, route_weight, returned[2:], CHUNKS[2:], early, jnp.bfloat16)
     return (mixed_out, expert_mix)
 
 
@@ -236,7 +335,7 @@
         P("ep", "tp", None),
     )
     return jax.shard_map(
-        shards,
+        body,
         mesh=mesh,
         in_specs=placed,
         out_specs=(P("ep", "tp"), P(("ep", "tp"), None)),

time: 421 us -> 342 us (0.81)
  the two profiles are of different devices: /device:TPU:121 before, /device:TPU:1 now
where the time goes in v2:
time: 342 us; the launch traced here: 341 us
  Pallas kernels  98.6 us (29%)
  waiting for transfers between devices  87 us (25%)
  blocking collectives  71.3 us (21%)
  starting transfers between devices  56.4 us (16%)
  between operations  14.4 us (4%)
  local copies, waits for them, and re-layouts  10.5 us (3%)
    ppermute x18, waiting for transfers between devices, send(): lax.ppermute(value, 'tp', [(i, (i + step) % size) for i in range(size)])  72.9 us
    all_to_all x3, blocking collectives, exchange(): return lax.all_to_all(value, 'ep', split_axis=0, concat_axis=0, tiled=True)  71.3 us
    pallas_call x9, Pallas kernels, expert(): pl.pallas_call(functools.partial(expert_kernel, sizes=sizes, addends=tupl...  50.9 us
    pallas_call x1, Pallas kernels, attention(): pl.pallas_call(attention_kernel, grid=(groups,), in_specs=[pl.BlockSpec(m...  37.5 us
    ppermute x18, starting transfers between devices, send(): lax.ppermute(value, 'tp', [(i, (i + step) % size) for i in range(size)])  24.1 us
    all_to_all x3, starting transfers between devices, exchange(): return lax.all_to_all(value, 'ep', split_axis=0, concat_axis=0, tiled=True)  21.8 us
    ppermute x2, waiting for transfers between devices, swap_ends(): return lax.ppermute(value, 'ep', [(i, size - 1 - i) for i in range(size)])  14.1 us
    ppermute x2, starting transfers between devices, swap_ends(): return lax.ppermute(value, 'ep', [(i, size - 1 - i) for i in range(size)])  10.3 us
  transfers between devices with their start and end apart: 24, of which 4 were waited for; matrix products, arithmetic and copies ran while one was open for 1% of the time, Pallas kernels for 28%

profile of v2, /device:TPU:1, one launch (start us, length us, event | category | flops | bytes accessed | tf_op | source)
XLA Modules:
  0.0 341.1 jit_solution(9901353032852419856)
XLA Ops:
  7.2 3.3 dispatch.1
  10.5 26.8 %all_to_all.67 = bf16[32,8,2048]{2,1,0:T(8,128)(2,1)S(1)} all-to-all(bf16[32,8,2048]{2,1,0:T(8,128)(2,1)} %bitcast.61), channel_id=1, replica_groups=mesh['ep'=32,'tp'=4] {'ep'}, dimensions={0} | all-to-all | bytes 2097152 | tf_op jit(solution)/shard_map/all_to_all | solution.py:261
  37.3 0.8 pad_maximum_fusion.1
  38.1 2.5 collective-permute-start.14
  40.6 24.2 %all_to_all.68 = bf16[32,8,2048]{2,1,0:T(8,128)(2,1)S(1)} all-to-all(bf16[32,8,2048]{2,1,0:T(8,128)(2,1)S(1)} %bitcast.60), channel_id=1, replica_groups=mesh['ep'=32,'tp'=4] {'ep'}, dimensions={0} | all-to-all | bytes 2097152 | tf_op jit(solution)/shard_map/all_to_all | solution.py:261
  64.9 2.7 collective-permute-start.15
  67.6 1.2 all_to_all.46
  68.8 20.3 %all_to_all.69 = bf16[32,4,2048]{2,1,0:T(4,128)(2,1)S(1)} all-to-all(bf16[32,4,2048]{2,1,0:T(4,128)(2,1)S(1)} %all_to_all.46), channel_id=1, replica_groups=mesh['ep'=32,'tp'=4] {'ep'}, dimensions={0} | all-to-all | bytes 1048576 | tf_op jit(solution)/shard_map/all_to_all | solution.py:261
  89.3 1.4 collective-permute-start.17
  90.8 7.1 %expert.15 = (bf16[256,2048]{1,0:T(8,128)(2,1)}, bf16[256,2048]{1,0:T(8,128)(2,1)}) custom-call(bf16[2048,512]{1,0:T(8,128)(2,1)} %bitcast.23, bf16[2048,512]{1,0:T(8,128)(2,1)} %bitcast.32, bf16[512,2048]{1,0:T(8,128)(2,1)} %bitcast.41, bf16[256,2048]{1,0:T(8,128)(2,1)} %collective-permute-done.15.refs_0_, bf16[256,2048]{1,0:T(8,128)(2,1)} %collective-permute-done.14.refs_1_), custom_call_target="tpu_custom_call" | custom-call | flops 3221225472 | bytes 6291456 | tf_op jit(solution)/shard_map/expert/pallas_call | solution.py:223
  98.0 2.7 collective-permute-start.18
  100.9 3.3 collective-permute-start.3
  104.2 30.5 %collective-permute-done.3.refs_0_ = bf16[128,2048]{1,0:T(8,128)(2,1)S(1)} collective-permute-done((bf16[128,2048]{1,0:T(8,128)(2,1)S(1)}, bf16[128,2048]{1,0:T(8,128)(2,1)S(1)}, u32[]{:S(2)}, u32[]{:S(2)}) %collective-permute-start.3) | collective-permute-done | bytes 524320 | tf_op jit(solution)/shard_map/ppermute | solution.py:252
  134.8 0.8 copy-done.8
  135.6 5.5 %expert.9 = (bf16[128,2048]{1,0:T(8,128)(2,1)}, bf16[128,2048]{1,0:T(8,128)(2,1)}) custom-call(bf16[2048,512]{1,0:T(8,128)(2,1)} %bitcast.24, bf16[2048,512]{1,0:T(8,128)(2,1)} %bitcast.33, bf16[512,2048]{1,0:T(8,128)(2,1)} %bitcast.42, bf16[128,2048]{1,0:T(8,128)(2,1)} %copy-done.8, bf16[128,2048]{1,0:T(8,128)(2,1)} %copy-done.7), custom_call_target="tpu_custom_call" | custom-call | flops 1610612736 | bytes 6291456 | tf_op jit(solution)/shard_map/expert/pallas_call | solution.py:223
  141.1 1.8 collective-permute-start.6
  142.9 7.1 %expert.12 = (bf16[256,2048]{1,0:T(8,128)(2,1)}, bf16[256,2048]{1,0:T(8,128)(2,1)}) custom-call(bf16[2048,512]{1,0:T(8,128)(2,1)} %bitcast.25, bf16[2048,512]{1,0:T(8,128)(2,1)} %bitcast.34, bf16[512,2048]{1,0:T(8,128)(2,1)} %bitcast.43, bf16[256,2048]{1,0:T(8,128)(2,1)} %collective-permute-done.9.refs_0_, bf16[256,2048]{1,0:T(8,128)(2,1)} %collective-permute-done.8.refs_1_), custom_call_target="tpu_custom_call" | custom-call | flops 3221225472 | bytes 6291456 | tf_op jit(solution)/shard_map/expert/pallas_call | solution.py:223
  150.1 2.7 collective-permute-start.11
  152.8 5.3 %expert.16 = bf16[256,2048]{1,0:T(8,128)(2,1)} custom-call(bf16[2048,512]{1,0:T(8,128)(2,1)} %bitcast.26, bf16[2048,512]{1,0:T(8,128)(2,1)} %bitcast.35, bf16[512,2048]{1,0:T(8,128)(2,1)} %bitcast.44, bf16[256,2048]{1,0:T(8,128)(2,1)} %collective-permute-done.17.refs_0_, bf16[256,2048]{1,0:T(8,128)(2,1)} %collective-permute-done.18.refs_1_), custom_call_target="tpu_custom_call" | custom-call | flops 1610612736 | bytes 6291456 | tf_op jit(solution)/shard_map/expert/pallas_call | solution.py:223
  158.2 2.7 collective-permute-start.19
  161.0 4.5 %expert.10 = bf16[128,2048]{1,0:T(8,128)(2,1)} custom-call(bf16[2048,512]{1,0:T(8,128)(2,1)} %bitcast.27, bf16[2048,512]{1,0:T(8,128)(2,1)} %bitcast.36, bf16[512,2048]{1,0:T(8,128)(2,1)} %bitcast.45, bf16[128,2048]{1,0:T(8,128)(2,1)} %collective-permute-done.5.refs_0_, bf16[128,2048]{1,0:T(8,128)(2,1)} %copy-done.11), custom_call_target="tpu_custom_call" | custom-call | flops 805306368 | bytes 6291456 | tf_op jit(solution)/shard_map/expert/pallas_call | solution.py:223
  165.4 1.4 collective-permute-start.7
  166.9 42.1 %collective-permute-done.7.refs_2_ = bf16[128,2048]{1,0:T(8,128)(2,1)S(1)} collective-permute-done((bf16[128,2048]{1,0:T(8,128)(2,1)}, bf16[128,2048]{1,0:T(8,128)(2,1)S(1)}, u32[]{:S(2)}, u32[]{:S(2)}) %collective-permute-start.7) | collective-permute-done | bytes 524320 | tf_op jit(solution)/shard_map/ppermute | solution.py:252
  209.0 0.8 copy-done.10
  209.8 4.7 %expert.11 = bf16[128,2048]{1,0:T(8,128)(2,1)} custom-call(bf16[2048,512]{1,0:T(8,128)(2,1)} %bitcast.28, bf16[2048,512]{1,0:T(8,128)(2,1)} %bitcast.37, bf16[512,2048]{1,0:T(8,128)(2,1)} %bitcast.46, bf16[128,2048]{1,0:T(8,128)(2,1)} %copy-done.4, bf16[128,2048]{1,0:T(8,128)(2,1)} %copy-done.9, bf16[128,2048]{1,0:T(8,128)(2,1)} %copy-done.10), custom_call_target="tpu_custom_call" | custom-call | flops 805306368 | bytes 6291456 | tf_op jit(solution)/shard_map/expert/pallas_call | solution.py:223
  214.5 2.0 all_to_all.49
  216.6 10.1 %all-to-all-start.2 = ((bf16[32,4,2048]{2,1,0:T(4,128)(2,1)}), bf16[32,4,2048]{2,1,0:T(4,128)(2,1)S(1)}, u32[]{:S(2)}, u32[]{:S(2)}) async-start(bf16[32,4,2048]{2,1,0:T(4,128)(2,1)} %all_to_all.49), calls=%async_computation.2 | async-start | bytes 1048576 | tf_op jit(solution)/shard_map/all_to_all | solution.py:261
  226.7 2.2 collective-permute-start.10
  228.9 5.3 %expert.13 = bf16[256,2048]{1,0:T(8,128)(2,1)} custom-call(bf16[2048,512]{1,0:T(8,128)(2,1)} %bitcast.29, bf16[2048,512]{1,0:T(8,128)(2,1)} %bitcast.38, bf16[512,2048]{1,0:T(8,128)(2,1)} %bitcast.47, bf16[256,2048]{1,0:T(8,128)(2,1)} %collective-permute-done.11.refs_0_, bf16[256,2048]{1,0:T(8,128)(2,1)} %collective-permute-done.12.refs_1_), custom_call_target="tpu_custom_call" | custom-call | flops 1610612736 | bytes 6291456 | tf_op jit(solution)/shard_map/expert/pallas_call | solution.py:223
  234.5 5.7 %expert.17 = bf16[256,2048]{1,0:T(8,128)(2,1)} custom-call(bf16[2048,512]{1,0:T(8,128)(2,1)} %bitcast.30, bf16[2048,512]{1,0:T(8,128)(2,1)} %bitcast.39, bf16[512,2048]{1,0:T(8,128)(2,1)} %bitcast.48, bf16[256,2048]{1,0:T(8,128)(2,1)} %bitcast.55, bf16[256,2048]{1,0:T(8,128)(2,1)} %collective-permute-done.16.refs_1_, ...), custom_call_target="tpu_custom_call" | custom-call | flops 1610612736 | bytes 6291456 | tf_op jit(solution)/shard_map/expert/pallas_call | solution.py:223
  240.2 7.8 %all-to-all-start.5 = ((bf16[32,8,2048]{2,1,0:T(8,128)(2,1)}), bf16[32,8,2048]{2,1,0:T(8,128)(2,1)S(1)}, u32[]{:S(2)}, u32[]{:S(2)}) async-start(bf16[32,8,2048]{2,1,0:T(8,128)(2,1)} %bitcast.57), calls=%async_computation.5 | async-start | bytes 2097152 | tf_op jit(solution)/shard_map/all_to_all | solution.py:261
  248.1 5.1 %collective-permute-start = (bf16[256,256]{1,0:T(8,128)(2,1)S(1)}, bf16[256,256]{1,0:T(8,128)(2,1)S(1)}, u32[]{:S(2)}, u32[]{:S(2)}) collective-permute-start(bf16[256,256]{1,0:T(8,128)(2,1)S(1)} %get-tuple-element.29), channel_id=1, source_target_pairs={{0,124},{4,120},{8,116},{12,112},{16,108},{20,104},{24,100},{28,96... | collective-permute-start | bytes 393224 | tf_op jit(solution)/shard_map/ppermute | solution.py:257
  253.2 0.6 pad_add_fusion.start_ref
  253.9 14.1 %collective-permute-done = bf16[256,256]{1,0:T(8,128)(2,1)S(1)} collective-permute-done((bf16[256,256]{1,0:T(8,128)(2,1)S(1)}, bf16[256,256]{1,0:T(8,128)(2,1)S(1)}, u32[]{:S(2)}, u32[]{:S(2)}) %collective-permute-start) | collective-permute-done | bytes 131104 | tf_op jit(solution)/shard_map/ppermute | solution.py:257
  267.9 0.7 pad_maximum_fusion.query_ref
  268.7 1.0 copy-done.5
  269.7 5.7 %expert.14 = bf16[256,2048]{1,0:T(8,128)(2,1)} custom-call(bf16[2048,512]{1,0:T(8,128)(2,1)} %bitcast.31, bf16[2048,512]{1,0:T(8,128)(2,1)} %bitcast.40, bf16[512,2048]{1,0:T(8,128)(2,1)} %bitcast.49, bf16[256,2048]{1,0:T(8,128)(2,1)} %bitcast.52, bf16[256,2048]{1,0:T(8,128)(2,1)} %copy-done.5, bf16[256,2048]{1,0:T(8,128)(2,1)} %collective-permute-done.13.refs_2_), custom_call_target="tpu_custom_call" | custom-call | flops 1610612736 | bytes 6291456 | tf_op jit(solution)/shard_map/expert/pallas_call | solution.py:223
  275.5 3.9 %all-to-all-start.4 = ((bf16[32,8,2048]{2,1,0:T(8,128)(2,1)}), bf16[32,8,2048]{2,1,0:T(8,128)(2,1)S(1)}, u32[]{:S(2)}, u32[]{:S(2)}) async-start(bf16[32,8,2048]{2,1,0:T(8,128)(2,1)} %bitcast.58), calls=%async_computation.4 | async-start | bytes 2097152 | tf_op jit(solution)/shard_map/all_to_all | solution.py:261
  279.4 37.5 %attention.1 = bf16[2,256,256]{2,1,0:T(8,128)(2,1)} custom-call(s32[2]{0:T(128)} %pad_add_fusion.start_ref, f32[2]{0:T(128)} %lambda_ref.1, f32[1,128]{1,0:T(1,128)} %bitcast.65, bf16[2,256,256]{2,1,0:T(8,128)(2,1)} %pad_maximum_fusion.query_ref, bf16[16384,256]{1,0:T(8,128)(2,1)} %all-gather.2.cloned.1.call-done.key_value_ref), custom_call_target="tpu_custom_call" | custom-call | flops 17999998976 | bytes 9000000 | tf_op jit(solution)/shard_map/attention/pallas_call | solution.py:69
  317.0 1.0 slice_bitcast_fusion.1
  317.9 5.2 %collective-permute-start.1 = (bf16[256,256]{1,0:T(8,128)(2,1)S(1)}, bf16[256,256]{1,0:T(8,128)(2,1)S(1)}, u32[]{:S(2)}, u32[]{:S(2)}) collective-permute-start(bf16[256,256]{1,0:T(8,128)(2,1)S(1)} %get-tuple-element.27), channel_id=1, source_target_pairs={{0,124},{4,120},{8,116},{12,112},{16,108},{20,104},{24,100},{28,96... | collective-permute-start | bytes 393224 | tf_op jit(solution)/shard_map/ppermute | solution.py:257
  323.2 0.7 copy.16.routes_ref
  323.9 0.7 copy.17.weight_ref
  324.6 0.9 all_to_all.51.refs_0_
  325.6 1.0 copy-done.3
  326.6 3.7 %combine.2.refs_1_ = f32[128,2048]{1,0:T(8,128)} custom-call(s32[128,4]{1,0:T(8,128)} %copy.16.routes_ref, f32[128,4]{1,0:T(8,128)} %copy.17.weight_ref, bf16[256,2048]{1,0:T(8,128)(2,1)} %bitcast.59, bf16[256,2048]{1,0:T(8,128)(2,1)} %bitcast.56), custom_call_target="tpu_custom_call" | custom-call | tf_op jit(solution)/shard_map/combine/pallas_call | solution.py:159
  330.3 3.2 combine.3
  333.5 0.7 pad_maximum_fusion.2
  (63 shorter events, 1.1 us)
Async XLA Ops:
  7.2 30.1 %copy-start.14 = (bf16[512,128]{1,0:T(8,128)(2,1)S(1)}, bf16[512,128]{1,0:T(8,128)(2,1)}, u32[]{:S(2)}) copy-start(bf16[512,128]{1,0:T(8,128)(2,1)} %param.13) | copy-start | bytes 393220
  7.2 30.1 %copy-start.13 = (bf16[512,128]{1,0:T(8,128)(2,1)S(1)}, bf16[512,128]{1,0:T(8,128)(2,1)}, u32[]{:S(2)}) copy-start(bf16[512,128]{1,0:T(8,128)(2,1)} %param.14) | copy-start | bytes 393220
  7.2 272.2 %all-gather.2.cloned.1.call-start = ((), (), s32[]{:S(2)}) async-start(), calls=%async_computation.6 | async-start | bytes 8650752 | tf_op jit(solution)/shard_map/all_gather | solution.py:296
  10.5 30.1 %copy-start.6 = (bf16[256,2048]{1,0:T(8,128)(2,1)S(1)}, bf16[256,2048]{1,0:T(8,128)(2,1)}, u32[]{:S(2)}) copy-start(bf16[256,2048]{1,0:T(8,128)(2,1)} %get-tuple-element.20) | copy-start | bytes 3145732
  37.3 52.0 %copy-start.1 = (bf16[32,8,2048]{2,1,0:T(8,128)(2,1)}, bf16[32,8,2048]{2,1,0:T(8,128)(2,1)S(1)}, u32[]{:S(2)}) copy-start(bf16[32,8,2048]{2,1,0:T(8,128)(2,1)S(1)} %all_to_all.67) | copy-start | bytes 3145732
  38.1 26.8 %collective-permute-start.14 = (bf16[256,2048]{1,0:T(8,128)(2,1)S(1)}, bf16[256,2048]{1,0:T(8,128)(2,1)}, u32[]{:S(2)}, u32[]{:S(2)}) collective-permute-start(bf16[256,2048]{1,0:T(8,128)(2,1)S(1)} %bitcast.53), channel_id=1, source_target_pairs={{0,3},{1,0},{2,1},{3,2},{4,7},{5,4},{6,5},{7,6},{8,11},{9,8},{10,9... | collective-permute-start | bytes 3145736 | tf_op jit(solution)/shard_map/ppermute | solution.py:252
  64.9 85.2 %copy-start = (bf16[32,8,2048]{2,1,0:T(8,128)(2,1)}, bf16[32,8,2048]{2,1,0:T(8,128)(2,1)S(1)}, u32[]{:S(2)}) copy-start(bf16[32,8,2048]{2,1,0:T(8,128)(2,1)S(1)} %all_to_all.68) | copy-start | bytes 3145732
  64.9 25.9 %collective-permute-start.8 = (bf16[256,2048]{1,0:T(8,128)(2,1)S(1)}, bf16[256,2048]{1,0:T(8,128)(2,1)}, u32[]{:S(2)}, u32[]{:S(2)}) collective-permute-start(bf16[256,2048]{1,0:T(8,128)(2,1)S(1)} %bitcast.50), channel_id=1, source_target_pairs={{0,1},{1,2},{2,3},{3,0},{4,5},{5,6},{6,7},{7,4},{8,9},{9,10},{10,1... | collective-permute-start | bytes 3145736 | tf_op jit(solution)/shard_map/ppermute | solution.py:252
  64.9 25.9 %collective-permute-start.15 = (bf16[256,2048]{1,0:T(8,128)(2,1)}, bf16[256,2048]{1,0:T(8,128)(2,1)}, u32[]{:S(2)}, u32[]{:S(2)}) collective-permute-start(bf16[256,2048]{1,0:T(8,128)(2,1)} %collective-permute-done.14.refs_1_), channel_id=1, source_target_pairs={{0,3},{1,0},{2,1},{3,2},{4,7},{5,4},{6,5},{7,6},{8,11},{9,8},{10,9... | collective-permute-start | bytes 3145736 | tf_op jit(solution)/shard_map/ppermute | solution.py:252
  89.2 15.0 %copy-start.4 = (bf16[128,2048]{1,0:T(8,128)(2,1)}, bf16[128,2048]{1,0:T(8,128)(2,1)S(1)}, u32[]{:S(2)}) copy-start(bf16[128,2048]{1,0:T(8,128)(2,1)S(1)} %all_to_all.48.refs_0_) | copy-start | bytes 1572868
  89.2 11.7 %collective-permute-start.2 = (bf16[128,2048]{1,0:T(8,128)(2,1)S(1)}, bf16[128,2048]{1,0:T(8,128)(2,1)S(1)}, u32[]{:S(2)}, u32[]{:S(2)}) collective-permute-start(bf16[128,2048]{1,0:T(8,128)(2,1)S(1)} %all_to_all.48.refs_0_), channel_id=1, source_target_pairs={{0,3},{1,0},{2,1},{3,2},{4,7},{5,4},{6,5},{7,6},{8,11},{9,8},{10,9... | collective-permute-start | bytes 1572872 | tf_op jit(solution)/shard_map/ppermute | solution.py:252
  89.3 60.7 %collective-permute-start.17 = (bf16[256,2048]{1,0:T(8,128)(2,1)S(1)}, bf16[256,2048]{1,0:T(8,128)(2,1)}, u32[]{:S(2)}, u32[]{:S(2)}) collective-permute-start(bf16[256,2048]{1,0:T(8,128)(2,1)S(1)} %bitcast.54), channel_id=1, source_target_pairs={{0,1},{1,2},{2,3},{3,0},{4,5},{5,6},{6,7},{7,4},{8,9},{9,10},{10,1... | collective-permute-start | bytes 3145736 | tf_op jit(solution)/shard_map/ppermute | solution.py:252
  90.7 52.2 %collective-permute-start.9 = (bf16[256,2048]{1,0:T(8,128)(2,1)}, bf16[256,2048]{1,0:T(8,128)(2,1)}, u32[]{:S(2)}, u32[]{:S(2)}) collective-permute-start(bf16[256,2048]{1,0:T(8,128)(2,1)} %collective-permute-done.8.refs_1_), channel_id=1, source_target_pairs={{0,1},{1,2},{2,3},{3,0},{4,5},{5,6},{6,7},{7,4},{8,9},{9,10},{10,1... | collective-permute-start | bytes 3145736 | tf_op jit(solution)/shard_map/ppermute | solution.py:252
  98.0 54.8 %collective-permute-start.18 = (bf16[256,2048]{1,0:T(8,128)(2,1)}, bf16[256,2048]{1,0:T(8,128)(2,1)}, u32[]{:S(2)}, u32[]{:S(2)}) collective-permute-start(bf16[256,2048]{1,0:T(8,128)(2,1)} %get-tuple-element.25), channel_id=1, source_target_pairs={{0,3},{1,0},{2,1},{3,2},{4,7},{5,4},{6,5},{7,6},{8,11},{9,8},{10,9... | collective-permute-start | bytes 3145736 | tf_op jit(solution)/shard_map/ppermute | solution.py:252
  100.9 33.9 %copy-start.7 = (bf16[128,2048]{1,0:T(8,128)(2,1)}, bf16[128,2048]{1,0:T(8,128)(2,1)S(1)}, u32[]{:S(2)}) copy-start(bf16[128,2048]{1,0:T(8,128)(2,1)S(1)} %collective-permute-done.2.refs_1_) | copy-start | bytes 1572868
  100.9 33.9 %collective-permute-start.3 = (bf16[128,2048]{1,0:T(8,128)(2,1)S(1)}, bf16[128,2048]{1,0:T(8,128)(2,1)S(1)}, u32[]{:S(2)}, u32[]{:S(2)}) collective-permute-start(bf16[128,2048]{1,0:T(8,128)(2,1)S(1)} %collective-permute-done.2.refs_1_), channel_id=1, source_target_pairs={{0,3},{1,0},{2,1},{3,2},{4,7},{5,4},{6,5},{7,6},{8,11},{9,8},{10,9... | collective-permute-start | bytes 1572872 | tf_op jit(solution)/shard_map/ppermute | solution.py:252
  104.2 53.9 %collective-permute-start.5 = (bf16[128,2048]{1,0:T(8,128)(2,1)S(1)}, bf16[128,2048]{1,0:T(8,128)(2,1)}, u32[]{:S(2)}, u32[]{:S(2)}) collective-permute-start(bf16[128,2048]{1,0:T(8,128)(2,1)S(1)} %all_to_all.48.refs_0_), channel_id=1, source_target_pairs={{0,1},{1,2},{2,3},{3,0},{4,5},{5,6},{6,7},{7,4},{8,9},{9,10},{10,1... | collective-permute-start | bytes 1572872 | tf_op jit(solution)/shard_map/ppermute | solution.py:252
  134.8 0.8 copy-start.8
  141.1 17.1 %collective-permute-start.6 = (bf16[128,2048]{1,0:T(8,128)(2,1)}, bf16[128,2048]{1,0:T(8,128)(2,1)S(1)}, u32[]{:S(2)}, u32[]{:S(2)}) collective-permute-start(bf16[128,2048]{1,0:T(8,128)(2,1)} %get-tuple-element.19), channel_id=1, source_target_pairs={{0,3},{1,0},{2,1},{3,2},{4,7},{5,4},{6,5},{7,6},{8,11},{9,8},{10,9... | collective-permute-start | bytes 1572872 | tf_op jit(solution)/shard_map/ppermute | solution.py:252
  142.9 22.5 %collective-permute-start.4 = (bf16[128,2048]{1,0:T(8,128)(2,1)}, bf16[128,2048]{1,0:T(8,128)(2,1)S(1)}, u32[]{:S(2)}, u32[]{:S(2)}) collective-permute-start(bf16[128,2048]{1,0:T(8,128)(2,1)} %get-tuple-element.18), channel_id=1, source_target_pairs={{0,1},{1,2},{2,3},{3,0},{4,5},{5,6},{6,7},{7,4},{8,9},{9,10},{10,1... | collective-permute-start | bytes 1572872 | tf_op jit(solution)/shard_map/ppermute | solution.py:252
  150.1 78.8 %collective-permute-start.11 = (bf16[256,2048]{1,0:T(8,128)(2,1)S(1)}, bf16[256,2048]{1,0:T(8,128)(2,1)}, u32[]{:S(2)}, u32[]{:S(2)}) collective-permute-start(bf16[256,2048]{1,0:T(8,128)(2,1)S(1)} %bitcast.51), channel_id=1, source_target_pairs={{0,3},{1,0},{2,1},{3,2},{4,7},{5,4},{6,5},{7,6},{8,11},{9,8},{10,9... | collective-permute-start | bytes 3145736 | tf_op jit(solution)/shard_map/ppermute | solution.py:252
  152.8 76.1 %collective-permute-start.12 = (bf16[256,2048]{1,0:T(8,128)(2,1)}, bf16[256,2048]{1,0:T(8,128)(2,1)}, u32[]{:S(2)}, u32[]{:S(2)}) collective-permute-start(bf16[256,2048]{1,0:T(8,128)(2,1)} %get-tuple-element.22), channel_id=1, source_target_pairs={{0,1},{1,2},{2,3},{3,0},{4,5},{5,6},{6,7},{7,4},{8,9},{9,10},{10,1... | collective-permute-start | bytes 3145736 | tf_op jit(solution)/shard_map/ppermute | solution.py:252
  158.1 76.3 %collective-permute-start.16 = (bf16[256,2048]{1,0:T(8,128)(2,1)}, bf16[256,2048]{1,0:T(8,128)(2,1)}, u32[]{:S(2)}, u32[]{:S(2)}) collective-permute-start(bf16[256,2048]{1,0:T(8,128)(2,1)} %get-tuple-element.24), channel_id=1, source_target_pairs={{0,1},{1,2},{2,3},{3,0},{4,5},{5,6},{6,7},{7,4},{8,9},{9,10},{10,1... | collective-permute-start | bytes 3145736 | tf_op jit(solution)/shard_map/ppermute | solution.py:252
  158.2 2.8 copy-start.11
  158.2 76.3 %collective-permute-start.19 = (bf16[256,2048]{1,0:T(8,128)(2,1)}, bf16[256,2048]{1,0:T(8,128)(2,1)}, u32[]{:S(2)}, u32[]{:S(2)}) collective-permute-start(bf16[256,2048]{1,0:T(8,128)(2,1)} %expert.16), channel_id=1, source_target_pairs={{0,3},{1,0},{2,1},{3,2},{4,7},{5,4},{6,5},{7,6},{8,11},{9,8},{10,9... | collective-permute-start | bytes 3145736 | tf_op jit(solution)/shard_map/ppermute | solution.py:252
  165.4 43.6 %copy-start.9 = (bf16[128,2048]{1,0:T(8,128)(2,1)}, bf16[128,2048]{1,0:T(8,128)(2,1)S(1)}, u32[]{:S(2)}) copy-start(bf16[128,2048]{1,0:T(8,128)(2,1)S(1)} %collective-permute-done.4.refs_1_) | copy-start | bytes 1572868
  165.4 43.6 %collective-permute-start.7 = (bf16[128,2048]{1,0:T(8,128)(2,1)}, bf16[128,2048]{1,0:T(8,128)(2,1)S(1)}, u32[]{:S(2)}, u32[]{:S(2)}) collective-permute-start(bf16[128,2048]{1,0:T(8,128)(2,1)} %expert.10), channel_id=1, source_target_pairs={{0,3},{1,0},{2,1},{3,2},{4,7},{5,4},{6,5},{7,6},{8,11},{9,8},{10,9... | collective-permute-start | bytes 1572872 | tf_op jit(solution)/shard_map/ppermute | solution.py:252
  209.0 0.8 copy-start.10
  216.6 23.7 %all-to-all-start.2 = ((bf16[32,4,2048]{2,1,0:T(4,128)(2,1)}), bf16[32,4,2048]{2,1,0:T(4,128)(2,1)S(1)}, u32[]{:S(2)}, u32[]{:S(2)}) async-start(bf16[32,4,2048]{2,1,0:T(4,128)(2,1)} %all_to_all.49), calls=%async_computation.2 | async-start | bytes 1048576 | tf_op jit(solution)/shard_map/all_to_all | solution.py:261
  226.7 41.9 %collective-permute-start.10 = (bf16[256,2048]{1,0:T(8,128)(2,1)}, bf16[256,2048]{1,0:T(8,128)(2,1)S(1)}, u32[]{:S(2)}, u32[]{:S(2)}) collective-permute-start(bf16[256,2048]{1,0:T(8,128)(2,1)} %get-tuple-element.21), channel_id=1, source_target_pairs={{0,3},{1,0},{2,1},{3,2},{4,7},{5,4},{6,5},{7,6},{8,11},{9,8},{10,9... | collective-permute-start | bytes 3145736 | tf_op jit(solution)/shard_map/ppermute | solution.py:252
  234.2 34.5 %collective-permute-start.13 = (bf16[256,2048]{1,0:T(8,128)(2,1)}, bf16[256,2048]{1,0:T(8,128)(2,1)}, u32[]{:S(2)}, u32[]{:S(2)}) collective-permute-start(bf16[256,2048]{1,0:T(8,128)(2,1)} %expert.13), channel_id=1, source_target_pairs={{0,1},{1,2},{2,3},{3,0},{4,5},{5,6},{6,7},{7,4},{8,9},{9,10},{10,1... | collective-permute-start | bytes 3145736 | tf_op jit(solution)/shard_map/ppermute | solution.py:252
  240.2 7.8 %copy-start.12 = (bf16[512,256]{1,0:T(8,128)(2,1)S(1)}, bf16[512,256]{1,0:T(8,128)(2,1)}, u32[]{:S(2)}) copy-start(bf16[512,256]{1,0:T(8,128)(2,1)} %param.12) | copy-start | bytes 786436
  240.2 35.2 %all-to-all-start.5 = ((bf16[32,8,2048]{2,1,0:T(8,128)(2,1)}), bf16[32,8,2048]{2,1,0:T(8,128)(2,1)S(1)}, u32[]{:S(2)}, u32[]{:S(2)}) async-start(bf16[32,8,2048]{2,1,0:T(8,128)(2,1)} %bitcast.57), calls=%async_computation.5 | async-start | bytes 2097152 | tf_op jit(solution)/shard_map/all_to_all | solution.py:261
  248.1 19.8 %collective-permute-start = (bf16[256,256]{1,0:T(8,128)(2,1)S(1)}, bf16[256,256]{1,0:T(8,128)(2,1)S(1)}, u32[]{:S(2)}, u32[]{:S(2)}) collective-permute-start(bf16[256,256]{1,0:T(8,128)(2,1)S(1)} %get-tuple-element.29), channel_id=1, source_target_pairs={{0,124},{4,120},{8,116},{12,112},{16,108},{20,104},{24,100},{28,96... | collective-permute-start | bytes 393224 | tf_op jit(solution)/shard_map/ppermute | solution.py:257
  268.6 1.0 copy-start.5
  275.4 41.5 %copy-start.2 = (bf16[32,8,2048]{2,1,0:T(8,128)(2,1)}, bf16[32,8,2048]{2,1,0:T(8,128)(2,1)S(1)}, u32[]{:S(2)}) copy-start(bf16[32,8,2048]{2,1,0:T(8,128)(2,1)S(1)} %all-to-all-done.5) | copy-start | bytes 3145732
  275.5 50.1 %all-to-all-start.4 = ((bf16[32,8,2048]{2,1,0:T(8,128)(2,1)}), bf16[32,8,2048]{2,1,0:T(8,128)(2,1)S(1)}, u32[]{:S(2)}, u32[]{:S(2)}) async-start(bf16[32,8,2048]{2,1,0:T(8,128)(2,1)} %bitcast.58), calls=%async_computation.4 | async-start | bytes 2097152 | tf_op jit(solution)/shard_map/all_to_all | solution.py:261
  279.4 43.8 %copy-start.15 = (s32[128,4]{0,1:T(4,128)S(1)}, s32[128,4]{0,1:T(4,128)}, u32[]{:S(2)}) copy-start(s32[128,4]{0,1:T(4,128)} %param.18) | copy-start | bytes 6148
  279.4 44.5 %copy-start.16 = (f32[128,4]{0,1:T(4,128)S(1)}, f32[128,4]{0,1:T(4,128)}, u32[]{:S(2)}) copy-start(f32[128,4]{0,1:T(4,128)} %param.19) | copy-start | bytes 6148
  317.9 15.6 %collective-permute-start.1 = (bf16[256,256]{1,0:T(8,128)(2,1)S(1)}, bf16[256,256]{1,0:T(8,128)(2,1)S(1)}, u32[]{:S(2)}, u32[]{:S(2)}) collective-permute-start(bf16[256,256]{1,0:T(8,128)(2,1)S(1)} %get-tuple-element.27), channel_id=1, source_target_pairs={{0,124},{4,120},{8,116},{12,112},{16,108},{20,104},{24,100},{28,96... | collective-permute-start | bytes 393224 | tf_op jit(solution)/shard_map/ppermute | solution.py:257
  325.6 1.0 copy-start.3
Sparse Core Ops, SparseCore 0:
  38.2 61.1 all-gather.1

commit v3 on v2

--- a/solution.py
+++ b/solution.py
@@ -12,13 +12,14 @@
 VDIM = 128
 LOG2E = 1.4426950408889634
 KEY_BLOCK = 1024
+SHARE = KEY_BLOCK // 2
 CHUNKS = ((0, 8), (8, 8), (16, 4))
-FAR_STEP = (1, -1, -1)
+GATHER_STEP = (1, -1, -1)
 
 epsilon = 1e-05
 
 
-def attention_kernel(start_ref, lambda_ref, gain_ref, query_ref, key_value_ref, out_ref, max_ref, sum_ref):
+def attention_kernel(start_ref, lambda_ref, gain_ref, query_ref, near_key, near_value, side_key, side_value, out_ref, max_ref, sum_ref):
     start = start_ref[pl.program_id(0)]
     rows = query_ref.shape[1]
     lane = lax.broadcasted_iota(jnp.int32, (rows, 2 * HEAD), 1)
@@ -27,10 +28,18 @@
     ones = jnp.ones((KEY_BLOCK, VDIM), jnp.bfloat16)
 
     def one_block(offset, masked):
-        keys = key_value_ref[pl.ds(offset, KEY_BLOCK), :2 * HEAD]
-        values = jnp.concatenate([key_value_ref[pl.ds(offset, KEY_BLOCK), 2 * HEAD:], ones], axis=1)
+        chip = offset // KEY_BLOCK
+        z_off = (chip // 4 + 4 - start_ref[3]) % 4
+        y_off = (chip % 4 + 4 - start_ref[4]) % 4
+        key_rows = pl.ds(pl.multiple_of((z_off * 4 + y_off) * SHARE, SHARE), SHARE)
+        value_rows = pl.ds(pl.multiple_of((y_off * 4 + z_off) * SHARE, SHARE), SHARE)
+        keys = jnp.concatenate([near_key[key_rows, :], side_key[key_rows, :]], axis=0)
+        values = jnp.concatenate([near_value[value_rows, :], side_value[value_rows, :]], axis=0)
+        values = jnp.concatenate([values, ones], axis=1)
         if masked:
-            column = lax.broadcasted_iota(jnp.int32, (rows, KEY_BLOCK), 1) + offset
+            column = lax.broadcasted_iota(jnp.int32, (rows, KEY_BLOCK), 1)
+            swapped = jnp.where(column < SHARE, column + SHARE, column - SHARE)
+            column = offset + jnp.where(start_ref[2] == 0, column, swapped)
             row = lax.broadcasted_iota(jnp.int32, (rows, KEY_BLOCK), 0) + start
             allowed = column <= row
         for which in range(4):
@@ -40,13 +49,13 @@
             scores = lax.dot_general(query, keys, (((1,), (1,)), ((), ())), preferred_element_type=jnp.float32)
             if masked:
                 scores = jnp.where(allowed, scores, -1e30)
-            old_max = max_ref[which]
+            old_max = max_ref[0, which]
             new_max = jnp.maximum(old_max, jnp.max(scores, axis=-1, keepdims=True))
             factor = jnp.exp2((old_max - new_max) * LOG2E)
             weights = jnp.exp2((scores - new_max) * LOG2E).astype(jnp.bfloat16)
             summed = jnp.dot(weights, values, preferred_element_type=jnp.float32)
-            sum_ref[which] = factor * sum_ref[which] + summed
-            max_ref[which] = new_max
+            sum_ref[0, which] = factor * sum_ref[0, which] + summed
+            max_ref[0, which] = new_max
 
     whole = start // KEY_BLOCK
 
@@ -57,7 +66,7 @@
     lax.fori_loop(0, whole, step, 0)
     one_block(pl.multiple_of(whole * KEY_BLOCK, KEY_BLOCK), True)
     for head in range(2):
-        first, second = sum_ref[head], sum_ref[2 + head]
+        first, second = sum_ref[0, head], sum_ref[0, 2 + head]
         combined = first[:, :VDIM] / first[:, VDIM:] - lambda_ref[head] * (second[:, :VDIM] / second[:, VDIM:])
         inverse = lax.rsqrt(jnp.mean(combined * combined, axis=-1, keepdims=True) + epsilon)
         out_ref[0, :, head * VDIM:(head + 1) * VDIM] = (combined * inverse * gain_ref[...]).astype(jnp.bfloat16)
@@ -65,7 +74,6 @@
 
 def attention(starts, head_lambda, out_gain, query_sets, keys_values):
     groups, rows, width = query_sets.shape
-    length, both = keys_values.shape
     return pl.pallas_call(
         attention_kernel,
         grid=(groups,),
@@ -74,18 +82,15 @@
             pl.BlockSpec(memory_space=pltpu.SMEM),
             pl.BlockSpec((1, VDIM), lambda g: (0, 0)),
             pl.BlockSpec((1, rows, width), lambda g: (g, 0, 0)),
-            pl.BlockSpec((length, both), lambda g: (0, 0)),
-        ],
+        ]
+        + [pl.BlockSpec(memory_space=pltpu.VMEM)] * 4,
         out_specs=pl.BlockSpec((1, rows, width), lambda g: (g, 0, 0)),
         out_shape=jax.ShapeDtypeStruct((groups, rows, width), jnp.bfloat16),
-        scratch_shapes=[
-            pltpu.VMEM((4, rows, 1), jnp.float32),
-            pltpu.VMEM((4, rows, 2 * VDIM), jnp.float32),
-        ],
+        scratch_shapes=[pltpu.VMEM((1, 4, rows, 1), jnp.float32), pltpu.VMEM((1, 4, rows, 2 * VDIM), jnp.float32)],
         compiler_params=pltpu.CompilerParams(vmem_limit_bytes=60 * 1024 * 1024),
         cost_estimate=pl.CostEstimate(flops=18_000_000_000, transcendentals=18_000_000, bytes_accessed=9_000_000),
         name="attention",
-    )(starts, head_lambda, out_gain, query_sets, keys_values)
+    )(starts, head_lambda, out_gain, query_sets, *keys_values)
 
 
 def dispatch_kernel(routes_ref, input_ref, gain_ref, *out_refs):
@@ -190,24 +195,31 @@
     used = 0
     for i in range(count):
         loads[i].wait()
-        rows = row_ref[pl.ds(begins[i], sizes[i]), :]
         if i == 0:
             gate_load.wait()
-        gate_pre = jnp.dot(rows, gate_ref[...], preferred_element_type=jnp.float32)
-        if i == 0:
             up_load.wait()
-        up_pre = jnp.dot(rows, up_ref[...], preferred_element_type=jnp.float32)
-        clipped = jnp.minimum(gate_pre, 7.0)
-        up_clip = jnp.clip(up_pre, -7.0, 7.0)
-        activated = ((up_clip + 1.0) * clipped * jax.nn.sigmoid(1.702 * clipped)).astype(jnp.bfloat16)
-        if i == 0:
             down_load.wait()
-        partial = jnp.dot(activated, down_ref[...], preferred_element_type=jnp.float32)
-        for j in range(used, used + addends[i]):
+        mine = range(used, used + addends[i])
+        for j in mine:
             extra_loads[j].wait()
-            partial = partial + extra_refs[j][...].astype(jnp.float32)
+        part = sizes[i] // 2
+
+        def half(index, carry, begin=begins[i], part=part, mine=mine):
+            here = pl.ds(pl.multiple_of(begin + index * part, part), part)
+            rows = row_ref[here, :]
+            gate_pre = jnp.dot(rows, gate_ref[...], preferred_element_type=jnp.float32)
+            up_pre = jnp.dot(rows, up_ref[...], preferred_element_type=jnp.float32)
+            clipped = jnp.minimum(gate_pre, 7.0)
+            up_clip = jnp.clip(up_pre, -7.0, 7.0)
+            activated = ((up_clip + 1.0) * clipped * jax.nn.sigmoid(1.702 * clipped)).astype(jnp.bfloat16)
+            partial = jnp.dot(activated, down_ref[...], preferred_element_type=jnp.float32)
+            for j in mine:
+                partial = partial + extra_refs[j][pl.ds(pl.multiple_of(index * part, part), part), :].astype(jnp.float32)
+            out_ref[here, :] = partial.astype(jnp.bfloat16)
+            return carry
+
+        lax.fori_loop(0, 2, half, 0)
         used += addends[i]
-        out_ref[pl.ds(begins[i], sizes[i]), :] = partial.astype(jnp.bfloat16)
         store = pltpu.make_async_copy(out_ref.at[pl.ds(begins[i], sizes[i]), :], out_hbm[i], out_sem.at[i])
         store.start()
         stores.append(store)
@@ -257,6 +269,24 @@
     return lax.ppermute(value, "ep", [(i, size - 1 - i) for i in range(size)])
 
 
+def around(value, stride):
+    size = lax.axis_size("ep")
+
+    def shift(part, step):
+        moved = [(i, i + ((i // stride + step) % 4 - i // stride % 4) * stride) for i in range(size)]
+        return lax.ppermute(part, "ep", moved)
+
+    behind = shift(value, 1)
+    ahead = shift(value, -1)
+    far = shift(behind, 1)
+    return jnp.concatenate([value, ahead, far, behind], axis=0)
+
+
+def sibling(value):
+    size = lax.axis_size("ep")
+    return lax.ppermute(value, "ep", [(i, i + 1 - 2 * (i % 2)) for i in range(size)])
+
+
 def exchange(value):
     return lax.all_to_all(value, "ep", split_axis=0, concat_axis=0, tiled=True)
 
@@ -285,34 +315,45 @@
     )
 
     other_queries = swap_ends(queries[half:])
+    near_key = around(around(keys, 2), 8)
+    near_value = around(around(values, 8), 2)
+    both = (near_key, near_value, sibling(near_key), sibling(near_value))
     outgoing = dispatch(routes, expert_input, moe_gain, ep_count)
 
     gathered = []
-    for name, rows, way in zip("abc", outgoing, FAR_STEP):
+    for rows, way in zip(outgoing, GATHER_STEP):
         mine = exchange(rows)
-        if name == "b":
-            keys, values, mine = lax.optimization_barrier((keys, values, mine))
-            both = jnp.concatenate([keys, values], axis=1)
-            both = lax.all_gather(both, "ep", axis=0, tiled=True)
         behind = send(mine, way)
         ahead = send(mine, -way)
         far = send(behind, way)
         gathered.append((mine, behind, ahead, far))
 
-    starts = jnp.stack([2 * half * me, 2 * half * partner + half]).astype(jnp.int32)
+    starts = jnp.stack([2 * half * me, 2 * half * partner + half, me % 2, me // 8, me // 2 % 4]).astype(jnp.int32)
     query_sets = jnp.stack([queries[:half], other_queries])
     mixed = attention(starts, head_lambda, out_gain.reshape(1, -1), query_sets, both)
     mixed_out = jnp.concatenate([mixed[0], swap_ends(mixed[1])], axis=0)
 
-    returned = []
-    for (mine, behind, ahead, far), way in zip(gathered, FAR_STEP):
-        for_far, for_behind = expert([far, behind], weights, [[], []])
-        passing = send(for_far, way)
-        from_ahead = send(for_behind, -way)
-        (for_ahead,) = expert([ahead], weights, [[passing]])
-        from_behind = send(for_ahead, way)
-        (own,) = expert([mine], weights, [[from_ahead, from_behind]])
-        returned.append(exchange(own))
+    def call(rows, addends):
+        return expert(rows, weights, addends)
+
+    (a_mine, a_behind, a_ahead, a_far), (b_mine, b_behind, b_ahead, b_far), (c_mine, c_behind, c_ahead, c_far) = gathered
+    c_behind, c_ahead = c_ahead, c_behind
+    way_a, way_b, way_c = 1, -1, 1
+
+    for_far, for_behind = call([a_far, a_behind], [[], []])
+    passing_a, a_first = send(for_far, way_a), send(for_behind, -way_a)
+    for_far, for_behind = call([b_far, b_behind], [[], []])
+    passing_b, b_first = send(for_far, way_b), send(for_behind, -way_b)
+    (for_ahead,) = call([a_ahead], [[passing_a]])
+    a_second = send(for_ahead, way_a)
+    for_ahead, for_far, for_behind = call([b_ahead, c_far, c_behind], [[passing_b], [], []])
+    b_second = send(for_ahead, way_b)
+    passing_c, c_first = send(for_far, way_c), send(for_behind, -way_c)
+    (own_a,) = call([a_mine], [[a_first, a_second]])
+    own_b, for_ahead = call([b_mine, c_ahead], [[b_first, b_second], [passing_c]])
+    c_second = send(for_ahead, way_c)
+    (own_c,) = call([c_mine], [[c_first, c_second]])
+    returned = [exchange(own_a), exchange(own_b), exchange(own_c)]
 
     early = combine(routes, route_weight, returned[:2], CHUNKS[:2], None, jnp.float32)
     expert_mix = combine(routes, route_weight, returned[2:], CHUNKS[2:], early, jnp.bfloat16)

time: 342 us -> 358 us (1.047)
  the two profiles are of different devices: /device:TPU:1 before, /device:TPU:121 now
where the time goes in v3:
time: 358 us; the launch traced here: 354 us
  Pallas kernels  107 us (30%)
  waiting for transfers between devices  95.1 us (27%)
  starting transfers between devices  80.3 us (22%)
  blocking collectives  42.4 us (12%)
  local copies, waits for them, and re-layouts  27 us (8%)
    ppermute x18, waiting for transfers between devices, send(): lax.ppermute(value, 'tp', [(i, (i + step) % size) for i in range(size)])  63.1 us
    pallas_call x7, Pallas kernels, expert(): pl.pallas_call(functools.partial(expert_kernel, sizes=sizes, addends=tupl...  59.3 us
    all_to_all x2, blocking collectives, exchange(): return lax.all_to_all(value, 'ep', split_axis=0, concat_axis=0, tiled=True)  42.4 us
    pallas_call x1, Pallas kernels, attention(): pl.pallas_call(attention_kernel, grid=(groups,), in_specs=[pl.BlockSpec(m...  37.7 us
    all_to_all x4, starting transfers between devices, exchange(): return lax.all_to_all(value, 'ep', split_axis=0, concat_axis=0, tiled=True)  32.1 us
    ppermute x18, starting transfers between devices, send(): lax.ppermute(value, 'tp', [(i, (i + step) % size) for i in range(size)])  21 us
    ppermute x2, waiting for transfers between devices, swap_ends(): return lax.ppermute(value, 'ep', [(i, size - 1 - i) for i in range(size)])  19.9 us
    unnamed x54, local copies, waits for them, and re-layouts  16.5 us
  transfers between devices with their start and end apart: 38, of which 8 were waited for; matrix products, arithmetic and copies ran while one was open for 6% of the time, Pallas kernels for 28%

profile of v3, /device:TPU:121, one launch (start us, length us, event | category | flops | bytes accessed | tf_op | source)
XLA Modules:
  0.0 354.5 jit_solution(11320203599819539367)
XLA Ops:
  0.6 3.2 dispatch.1
  3.9 21.7 %all_to_all.66 = bf16[32,8,2048]{2,1,0:T(8,128)(2,1)S(1)} all-to-all(bf16[32,8,2048]{2,1,0:T(8,128)(2,1)} %bitcast.58), channel_id=1, replica_groups=mesh['ep'=32,'tp'=4] {'ep'}, dimensions={0} | all-to-all | bytes 2097152 | tf_op jit(solution)/shard_map/all_to_all | solution.py:291
  26.8 20.7 %all_to_all.67 = bf16[32,8,2048]{2,1,0:T(8,128)(2,1)S(1)} all-to-all(bf16[32,8,2048]{2,1,0:T(8,128)(2,1)S(1)} %bitcast.57), channel_id=1, replica_groups=mesh['ep'=32,'tp'=4] {'ep'}, dimensions={0} | all-to-all | bytes 2097152 | tf_op jit(solution)/shard_map/all_to_all | solution.py:291
  47.5 1.5 collective-permute-start.20
  48.9 3.0 collective-permute-done.28.refs_1_
  52.0 2.7 collective-permute-start.2
  54.7 1.4 collective-permute-start.8
  57.2 7.7 %all-to-all-start = ((bf16[32,4,2048]{2,1,0:T(4,128)(2,1)}), bf16[32,4,2048]{2,1,0:T(4,128)(2,1)S(1)}, u32[]{:S(2)}, u32[]{:S(2)}) async-start(bf16[32,4,2048]{2,1,0:T(4,128)(2,1)} %all_to_all.42), calls=%async_computation | async-start | bytes 1048576 | tf_op jit(solution)/shard_map/all_to_all | solution.py:291
  67.0 2.1 collective-permute-start.9
  69.9 4.9 %collective-permute-done.7 = bf16[512,128]{1,0:T(8,128)(2,1)S(1)} collective-permute-done((bf16[512,128]{1,0:T(8,128)(2,1)S(1)}, bf16[512,128]{1,0:T(8,128)(2,1)S(1)}, u32[]{:S(2)}, u32[]{:S(2)}) %collective-permute-start.7) | collective-permute-done | bytes 131104 | tf_op jit(solution)/shard_map/ppermute | solution.py:277
  77.9 1.7 collective-permute-start.5
  82.3 2.6 collective-permute-start.31
  85.0 8.8 %expert.11 = (bf16[256,2048]{1,0:T(8,128)(2,1)}, bf16[256,2048]{1,0:T(8,128)(2,1)}) custom-call(bf16[2048,512]{1,0:T(8,128)(2,1)} %bitcast.26, bf16[2048,512]{1,0:T(8,128)(2,1)} %bitcast.33, bf16[512,2048]{1,0:T(8,128)(2,1)} %bitcast.40, bf16[256,2048]{1,0:T(8,128)(2,1)} %collective-permute-done.29.refs_0_, bf16[256,2048]{1,0:T(8,128)(2,1)} %collective-permute-done.28.refs_1_), custom_call_target="tpu_custom_call" | custom-call | flops 3221225472 | bytes 6291456 | tf_op jit(solution)/shard_map/expert/pallas_call | solution.py:235
  94.5 1.4 collective-permute-start.32
  96.0 1.5 collective-permute-start.11
  97.5 1.3 collective-permute-start.17
  98.8 1.9 constant_dynamic-update-slice_fusion.6
  100.7 7.1 %collective-permute-done.11 = bf16[2048,128]{1,0:T(8,128)(2,1)S(1)} collective-permute-done((bf16[2048,128]{1,0:T(8,128)(2,1)}, bf16[2048,128]{1,0:T(8,128)(2,1)S(1)}, u32[]{:S(2)}, u32[]{:S(2)}) %collective-permute-start.11) | collective-permute-done | bytes 524320 | tf_op jit(solution)/shard_map/ppermute | solution.py:277
  108.1 31.8 %collective-permute-done.17.refs_1_ = bf16[128,2048]{1,0:T(8,128)(2,1)S(1)} collective-permute-done((bf16[128,2048]{1,0:T(8,128)(2,1)S(1)}, bf16[128,2048]{1,0:T(8,128)(2,1)S(1)}, u32[]{:S(2)}, u32[]{:S(2)}) %collective-permute-start.17) | collective-permute-done | bytes 524320 | tf_op jit(solution)/shard_map/ppermute | solution.py:264
  141.2 8.8 %expert.7 = (bf16[256,2048]{1,0:T(8,128)(2,1)}, bf16[256,2048]{1,0:T(8,128)(2,1)}) custom-call(bf16[2048,512]{1,0:T(8,128)(2,1)} %bitcast.27, bf16[2048,512]{1,0:T(8,128)(2,1)} %bitcast.34, bf16[512,2048]{1,0:T(8,128)(2,1)} %bitcast.41, bf16[256,2048]{1,0:T(8,128)(2,1)} %collective-permute-done.21.refs_0_, bf16[256,2048]{1,0:T(8,128)(2,1)} %collective-permute-done.20.refs_1_), custom_call_target="tpu_custom_call" | custom-call | flops 3221225472 | bytes 6291456 | tf_op jit(solution)/shard_map/expert/pallas_call | solution.py:235
  150.8 2.8 collective-permute-start.22
  153.5 1.9 constant_dynamic-update-slice_fusion.17
  155.4 6.7 %expert.12 = bf16[256,2048]{1,0:T(8,128)(2,1)} custom-call(bf16[2048,512]{1,0:T(8,128)(2,1)} %bitcast.28, bf16[2048,512]{1,0:T(8,128)(2,1)} %bitcast.35, bf16[512,2048]{1,0:T(8,128)(2,1)} %bitcast.42, bf16[256,2048]{1,0:T(8,128)(2,1)} %collective-permute-done.31.refs_0_, bf16[256,2048]{1,0:T(8,128)(2,1)} %collective-permute-done.32.refs_1_), custom_call_target="tpu_custom_call" | custom-call | flops 1610612736 | bytes 6291456 | tf_op jit(solution)/shard_map/expert/pallas_call | solution.py:235
  162.1 1.4 collective-permute-start.18
  163.7 1.4 collective-permute-start.33
  165.0 1.9 constant_dynamic-update-slice_fusion.5
  166.9 1.9 constant_dynamic-update-slice_fusion.4.near_key
  168.8 1.9 constant_dynamic-update-slice_fusion.16
  170.7 14.0 %collective-permute-done.18.refs_1_ = bf16[128,2048]{1,0:T(8,128)(2,1)S(1)} collective-permute-done((bf16[128,2048]{1,0:T(8,128)(2,1)S(1)}, bf16[128,2048]{1,0:T(8,128)(2,1)S(1)}, u32[]{:S(2)}, u32[]{:S(2)}) %collective-permute-start.18) | collective-permute-done | bytes 524320 | tf_op jit(solution)/shard_map/ppermute | solution.py:264
  184.7 6.9 %collective-permute-start.13 = (bf16[8192,128]{1,0:T(8,128)(2,1)}, bf16[8192,128]{1,0:T(8,128)(2,1)}, u32[]{:S(2)}, u32[]{:S(2)}) collective-permute-start(bf16[8192,128]{1,0:T(8,128)(2,1)} %constant_dynamic-update-slice_fusion.4.near_key), channel_id=1, source_target_pairs={{0,4},{4,0},{8,12},{12,8},{16,20},{20,16},{24,28},{28,24},{32,36},... | collective-permute-start | bytes 6291464 | tf_op jit(solution)/shard_map/ppermute | solution.py:287
  191.6 1.5 collective-permute-start.24
  193.1 12.0 %expert.8 = (bf16[256,2048]{1,0:T(8,128)(2,1)}, bf16[128,2048]{1,0:T(8,128)(2,1)}, bf16[128,2048]{1,0:T(8,128)(2,1)}) custom-call(bf16[2048,512]{1,0:T(8,128)(2,1)} %bitcast.29, bf16[2048,512]{1,0:T(8,128)(2,1)} %bitcast.36, bf16[512,2048]{1,0:T(8,128)(2,1)} %bitcast.43, bf16[256,2048]{1,0:T(8,128)(2,1)} %collective-permute-done.16.refs_0_, ...), custom_call_target="tpu_custom_call" | custom-call | flops 3221225472 | bytes 6291456 | tf_op jit(solution)/shard_map/expert/pallas_call | solution.py:235
  205.1 2.0 collective-permute-start.25
  207.9 5.7 %collective-permute-start.14 = (bf16[8192,128]{1,0:T(8,128)(2,1)}, bf16[8192,128]{1,0:T(8,128)(2,1)}, u32[]{:S(2)}, u32[]{:S(2)}) collective-permute-start(bf16[8192,128]{1,0:T(8,128)(2,1)} %constant_dynamic-update-slice_fusion.15.near_value), channel_id=1, source_target_pairs={{0,4},{4,0},{8,12},{12,8},{16,20},{20,16},{24,28},{28,24},{32,36},... | collective-permute-start | bytes 6291464 | tf_op jit(solution)/shard_map/ppermute | solution.py:287
  213.6 7.0 %expert.13 = bf16[256,2048]{1,0:T(8,128)(2,1)} custom-call(bf16[2048,512]{1,0:T(8,128)(2,1)} %bitcast.30, bf16[2048,512]{1,0:T(8,128)(2,1)} %bitcast.37, bf16[512,2048]{1,0:T(8,128)(2,1)} %bitcast.44, bf16[256,2048]{1,0:T(8,128)(2,1)} %bitcast.52, bf16[256,2048]{1,0:T(8,128)(2,1)} %copy-done.5, bf16[256,2048]{1,0:T(8,128)(2,1)} %collective-permute-done.33.refs_2_), custom_call_target="tpu_custom_call" | custom-call | flops 1610612736 | bytes 6291456 | tf_op jit(solution)/shard_map/expert/pallas_call | solution.py:235
  220.6 8.8 %all-to-all-start.4 = ((bf16[32,8,2048]{2,1,0:T(8,128)(2,1)}), bf16[32,8,2048]{2,1,0:T(8,128)(2,1)S(1)}, u32[]{:S(2)}, u32[]{:S(2)}) async-start(bf16[32,8,2048]{2,1,0:T(8,128)(2,1)} %bitcast.55), calls=%async_computation.4 | async-start | bytes 2097152 | tf_op jit(solution)/shard_map/all_to_all | solution.py:291
  230.6 14.3 %collective-permute-done.26.refs_4_ = bf16[128,2048]{1,0:T(8,128)(2,1)S(1)} collective-permute-done((bf16[128,2048]{1,0:T(8,128)(2,1)S(1)}, bf16[128,2048]{1,0:T(8,128)(2,1)S(1)}, u32[]{:S(2)}, u32[]{:S(2)}) %collective-permute-start.26) | collective-permute-done | bytes 524320 | tf_op jit(solution)/shard_map/ppermute | solution.py:264
  245.7 9.5 %expert.9 = (bf16[256,2048]{1,0:T(8,128)(2,1)}, bf16[128,2048]{1,0:T(8,128)(2,1)}) custom-call(bf16[2048,512]{1,0:T(8,128)(2,1)} %bitcast.31, bf16[2048,512]{1,0:T(8,128)(2,1)} %bitcast.38, bf16[512,2048]{1,0:T(8,128)(2,1)} %bitcast.45, bf16[256,2048]{1,0:T(8,128)(2,1)} %bitcast.49, bf16[128,2048]{1,0:T(8,128)(2,1)} %copy-done.8, ...), custom_call_target="tpu_custom_call" | custom-call | flops 2415919104 | bytes 6291456 | tf_op jit(solution)/shard_map/expert/pallas_call | solution.py:235
  255.2 8.1 %all-to-all-start.5 = ((bf16[32,8,2048]{2,1,0:T(8,128)(2,1)}), bf16[32,8,2048]{2,1,0:T(8,128)(2,1)S(1)}, u32[]{:S(2)}, u32[]{:S(2)}) async-start(bf16[32,8,2048]{2,1,0:T(8,128)(2,1)} %bitcast.56), calls=%async_computation.5 | async-start | bytes 2097152 | tf_op jit(solution)/shard_map/all_to_all | solution.py:291
  263.4 1.5 collective-permute-start.23
  266.9 12.7 %collective-permute-done = bf16[256,256]{1,0:T(8,128)(2,1)S(1)} collective-permute-done((bf16[256,256]{1,0:T(8,128)(2,1)}, bf16[256,256]{1,0:T(8,128)(2,1)S(1)}, u32[]{:S(2)}, u32[]{:S(2)}) %collective-permute-start) | collective-permute-done | bytes 131104 | tf_op jit(solution)/shard_map/ppermute | solution.py:269
  281.9 6.6 %expert.10 = bf16[128,2048]{1,0:T(8,128)(2,1)} custom-call(bf16[2048,512]{1,0:T(8,128)(2,1)} %bitcast.32, bf16[2048,512]{1,0:T(8,128)(2,1)} %bitcast.39, bf16[512,2048]{1,0:T(8,128)(2,1)} %bitcast.46, bf16[128,2048]{1,0:T(8,128)(2,1)} %copy-done.4, bf16[128,2048]{1,0:T(8,128)(2,1)} %copy-done.9, bf16[128,2048]{1,0:T(8,128)(2,1)} %copy-done.10), custom_call_target="tpu_custom_call" | custom-call | flops 805306368 | bytes 6291456 | tf_op jit(solution)/shard_map/expert/pallas_call | solution.py:235
  288.6 2.0 all_to_all.48
  290.6 7.6 %all-to-all-start.2 = ((bf16[32,4,2048]{2,1,0:T(4,128)(2,1)}), bf16[32,4,2048]{2,1,0:T(4,128)(2,1)S(1)}, u32[]{:S(2)}, u32[]{:S(2)}) async-start(bf16[32,4,2048]{2,1,0:T(4,128)(2,1)} %all_to_all.48), calls=%async_computation.2 | async-start | bytes 1048576 | tf_op jit(solution)/shard_map/all_to_all | solution.py:291
  298.2 37.7 %attention.1 = bf16[2,256,256]{2,1,0:T(8,128)(2,1)} custom-call(s32[5]{0:T(128)} %stack.32.start_ref, f32[2]{0:T(128)} %lambda_ref.1, f32[1,128]{1,0:T(1,128)} %bitcast.62, bf16[2,256,256]{2,1,0:T(8,128)(2,1)} %pad_maximum_fusion.query_ref, bf16[8192,128]{1,0:T(8,128)(2,1)} %constant_dynamic-update-slice_fusion.4.near_key, ...), custom_call_target="tpu_custom_call" | custom-call | flops 17999998976 | bytes 9000000 | tf_op jit(solution)/shard_map/attention/pallas_call | solution.py:77
  338.7 7.2 %collective-permute-done.15 = bf16[256,256]{1,0:T(8,128)(2,1)S(1)} collective-permute-done((bf16[256,256]{1,0:T(8,128)(2,1)S(1)}, bf16[256,256]{1,0:T(8,128)(2,1)S(1)}, u32[]{:S(2)}, u32[]{:S(2)}) %collective-permute-start.15) | collective-permute-done | bytes 131104 | tf_op jit(solution)/shard_map/ppermute | solution.py:269
  346.6 3.8 %combine.2.refs_1_ = f32[128,2048]{1,0:T(8,128)} custom-call(s32[128,4]{1,0:T(8,128)} %copy.16.routes_ref, f32[128,4]{1,0:T(8,128)} %copy.17.weight_ref, bf16[256,2048]{1,0:T(8,128)(2,1)} %bitcast.53, bf16[256,2048]{1,0:T(8,128)(2,1)} %bitcast.54), custom_call_target="tpu_custom_call" | custom-call | tf_op jit(solution)/shard_map/combine/pallas_call | solution.py:164
  351.3 3.2 combine.3
  (108 shorter events, 26.1 us)
Async XLA Ops:
  3.8 48.2 %copy-start.15 = (bf16[512,128]{1,0:T(8,128)(2,1)S(1)}, bf16[512,128]{1,0:T(8,128)(2,1)}, u32[]{:S(2)}) copy-start(bf16[512,128]{1,0:T(8,128)(2,1)} %param.13) | copy-start | bytes 393220
  3.9 50.9 %copy-start.16 = (bf16[512,128]{1,0:T(8,128)(2,1)S(1)}, bf16[512,128]{1,0:T(8,128)(2,1)}, u32[]{:S(2)}) copy-start(bf16[512,128]{1,0:T(8,128)(2,1)} %param.14) | copy-start | bytes 393220
  3.9 52.3 %copy-start.13 = (bf16[128,2048]{1,0:T(8,128)(2,1)S(1)}, bf16[128,2048]{1,0:T(8,128)(2,1)}, u32[]{:S(2)}) copy-start(bf16[128,2048]{1,0:T(8,128)(2,1)} %get-tuple-element.14) | copy-start | bytes 1572868
  25.6 56.7 %copy-start.1 = (bf16[32,8,2048]{2,1,0:T(8,128)(2,1)}, bf16[32,8,2048]{2,1,0:T(8,128)(2,1)S(1)}, u32[]{:S(2)}) copy-start(bf16[32,8,2048]{2,1,0:T(8,128)(2,1)S(1)} %all_to_all.66) | copy-start | bytes 3145732
  25.6 26.4 %collective-permute-start.28 = (bf16[256,2048]{1,0:T(8,128)(2,1)S(1)}, bf16[256,2048]{1,0:T(8,128)(2,1)}, u32[]{:S(2)}, u32[]{:S(2)}) collective-permute-start(bf16[256,2048]{1,0:T(8,128)(2,1)S(1)} %bitcast.50), channel_id=1, source_target_pairs={{0,1},{1,2},{2,3},{3,0},{4,5},{5,6},{6,7},{7,4},{8,9},{9,10},{10,1... | collective-permute-start | bytes 3145736 | tf_op jit(solution)/shard_map/ppermute | solution.py:264
  47.5 102.5 %copy-start = (bf16[32,8,2048]{2,1,0:T(8,128)(2,1)}, bf16[32,8,2048]{2,1,0:T(8,128)(2,1)S(1)}, u32[]{:S(2)}) copy-start(bf16[32,8,2048]{2,1,0:T(8,128)(2,1)S(1)} %all_to_all.67) | copy-start | bytes 3145732
  47.5 34.8 %collective-permute-start.20 = (bf16[256,2048]{1,0:T(8,128)(2,1)S(1)}, bf16[256,2048]{1,0:T(8,128)(2,1)}, u32[]{:S(2)}, u32[]{:S(2)}) collective-permute-start(bf16[256,2048]{1,0:T(8,128)(2,1)S(1)} %bitcast.47), channel_id=1, source_target_pairs={{0,3},{1,0},{2,1},{3,2},{4,7},{5,4},{6,5},{7,6},{8,11},{9,8},{10,9... | collective-permute-start | bytes 3145736 | tf_op jit(solution)/shard_map/ppermute | solution.py:264
  51.9 32.9 %collective-permute-start.29 = (bf16[256,2048]{1,0:T(8,128)(2,1)}, bf16[256,2048]{1,0:T(8,128)(2,1)}, u32[]{:S(2)}, u32[]{:S(2)}) collective-permute-start(bf16[256,2048]{1,0:T(8,128)(2,1)} %collective-permute-done.28.refs_1_), channel_id=1, source_target_pairs={{0,1},{1,2},{2,3},{3,0},{4,5},{5,6},{6,7},{7,4},{8,9},{9,10},{10,1... | collective-permute-start | bytes 3145736 | tf_op jit(solution)/shard_map/ppermute | solution.py:264
  52.0 13.5 %collective-permute-start.1 = (bf16[512,128]{1,0:T(8,128)(2,1)S(1)}, bf16[512,128]{1,0:T(8,128)(2,1)S(1)}, u32[]{:S(2)}, u32[]{:S(2)}) collective-permute-start(bf16[512,128]{1,0:T(8,128)(2,1)S(1)} %copy-done.15), channel_id=1, source_target_pairs={{0,24},{4,28},{8,0},{12,4},{16,8},{20,12},{24,16},{28,20},{32,56},... | collective-permute-start | bytes 393224 | tf_op jit(solution)/shard_map/ppermute | solution.py:277
  52.0 14.8 %collective-permute-start.2 = (bf16[512,128]{1,0:T(8,128)(2,1)S(1)}, bf16[512,128]{1,0:T(8,128)(2,1)S(1)}, u32[]{:S(2)}, u32[]{:S(2)}) collective-permute-start(bf16[512,128]{1,0:T(8,128)(2,1)S(1)} %copy-done.15), channel_id=1, source_target_pairs={{0,8},{4,12},{8,16},{12,20},{16,24},{20,28},{24,0},{28,4},{32,40},... | collective-permute-start | bytes 393224 | tf_op jit(solution)/shard_map/ppermute | solution.py:277
  54.7 12.3 %collective-permute-start.8 = (bf16[512,128]{1,0:T(8,128)(2,1)S(1)}, bf16[512,128]{1,0:T(8,128)(2,1)S(1)}, u32[]{:S(2)}, u32[]{:S(2)}) collective-permute-start(bf16[512,128]{1,0:T(8,128)(2,1)S(1)} %copy-done.16), channel_id=1, source_target_pairs={{0,32},{4,36},{8,40},{12,44},{16,48},{20,52},{24,56},{28,60},{32,6... | collective-permute-start | bytes 393224 | tf_op jit(solution)/shard_map/ppermute | solution.py:277
  57.2 38.7 %all-to-all-start = ((bf16[32,4,2048]{2,1,0:T(4,128)(2,1)}), bf16[32,4,2048]{2,1,0:T(4,128)(2,1)S(1)}, u32[]{:S(2)}, u32[]{:S(2)}) async-start(bf16[32,4,2048]{2,1,0:T(4,128)(2,1)} %all_to_all.42), calls=%async_computation | async-start | bytes 1048576 | tf_op jit(solution)/shard_map/all_to_all | solution.py:291
  65.5 9.2 %collective-permute-start.7 = (bf16[512,128]{1,0:T(8,128)(2,1)S(1)}, bf16[512,128]{1,0:T(8,128)(2,1)S(1)}, u32[]{:S(2)}, u32[]{:S(2)}) collective-permute-start(bf16[512,128]{1,0:T(8,128)(2,1)S(1)} %copy-done.16), channel_id=1, source_target_pairs={{0,96},{4,100},{8,104},{12,108},{16,112},{20,116},{24,120},{28,124... | collective-permute-start | bytes 393224 | tf_op jit(solution)/shard_map/ppermute | solution.py:277
  66.8 8.7 %collective-permute-start.3 = (bf16[512,128]{1,0:T(8,128)(2,1)S(1)}, bf16[512,128]{1,0:T(8,128)(2,1)S(1)}, u32[]{:S(2)}, u32[]{:S(2)}) collective-permute-start(bf16[512,128]{1,0:T(8,128)(2,1)S(1)} %collective-permute-done.2), channel_id=1, source_target_pairs={{0,8},{4,12},{8,16},{12,20},{16,24},{20,28},{24,0},{28,4},{32,40},... | collective-permute-start | bytes 393224 | tf_op jit(solution)/shard_map/ppermute | solution.py:277
  67.0 12.5 %collective-permute-start.9 = (bf16[512,128]{1,0:T(8,128)(2,1)S(1)}, bf16[512,128]{1,0:T(8,128)(2,1)S(1)}, u32[]{:S(2)}, u32[]{:S(2)}) collective-permute-start(bf16[512,128]{1,0:T(8,128)(2,1)S(1)} %collective-permute-done.8), channel_id=1, source_target_pairs={{0,32},{4,36},{8,40},{12,44},{16,48},{20,52},{24,56},{28,60},{32,6... | collective-permute-start | bytes 393224 | tf_op jit(solution)/shard_map/ppermute | solution.py:277
  76.9 16.9 %collective-permute-start.4 = (bf16[2048,128]{1,0:T(8,128)(2,1)}, bf16[2048,128]{1,0:T(8,128)(2,1)S(1)}, u32[]{:S(2)}, u32[]{:S(2)}) collective-permute-start(bf16[2048,128]{1,0:T(8,128)(2,1)} %get-tuple-element.38), channel_id=1, source_target_pairs={{0,96},{4,100},{8,104},{12,108},{16,112},{20,116},{24,120},{28,124... | collective-permute-start | bytes 1572872 | tf_op jit(solution)/shard_map/ppermute | solution.py:277
  77.9 18.1 %collective-permute-start.5 = (bf16[2048,128]{1,0:T(8,128)(2,1)}, bf16[2048,128]{1,0:T(8,128)(2,1)}, u32[]{:S(2)}, u32[]{:S(2)}) collective-permute-start(bf16[2048,128]{1,0:T(8,128)(2,1)} %get-tuple-element.38), channel_id=1, source_target_pairs={{0,32},{4,36},{8,40},{12,44},{16,48},{20,52},{24,56},{28,60},{32,6... | collective-permute-start | bytes 1572872 | tf_op jit(solution)/shard_map/ppermute | solution.py:277
  81.0 16.5 %collective-permute-start.10 = (bf16[2048,128]{1,0:T(8,128)(2,1)}, bf16[2048,128]{1,0:T(8,128)(2,1)}, u32[]{:S(2)}, u32[]{:S(2)}) collective-permute-start(bf16[2048,128]{1,0:T(8,128)(2,1)} %get-tuple-element.30), channel_id=1, source_target_pairs={{0,24},{4,28},{8,0},{12,4},{16,8},{20,12},{24,16},{28,20},{32,56},... | collective-permute-start | bytes 1572872 | tf_op jit(solution)/shard_map/ppermute | solution.py:277
  82.3 67.6 %collective-permute-start.31 = (bf16[256,2048]{1,0:T(8,128)(2,1)S(1)}, bf16[256,2048]{1,0:T(8,128)(2,1)}, u32[]{:S(2)}, u32[]{:S(2)}) collective-permute-start(bf16[256,2048]{1,0:T(8,128)(2,1)S(1)} %bitcast.51), channel_id=1, source_target_pairs={{0,3},{1,0},{2,1},{3,2},{4,7},{5,4},{6,5},{7,6},{8,11},{9,8},{10,9... | collective-permute-start | bytes 3145736 | tf_op jit(solution)/shard_map/ppermute | solution.py:264
  84.9 55.3 %collective-permute-start.21 = (bf16[256,2048]{1,0:T(8,128)(2,1)}, bf16[256,2048]{1,0:T(8,128)(2,1)}, u32[]{:S(2)}, u32[]{:S(2)}) collective-permute-start(bf16[256,2048]{1,0:T(8,128)(2,1)} %collective-permute-done.20.refs_1_), channel_id=1, source_target_pairs={{0,3},{1,0},{2,1},{3,2},{4,7},{5,4},{6,5},{7,6},{8,11},{9,8},{10,9... | collective-permute-start | bytes 3145736 | tf_op jit(solution)/shard_map/ppermute | solution.py:264
  94.5 56.2 %collective-permute-start.32 = (bf16[256,2048]{1,0:T(8,128)(2,1)}, bf16[256,2048]{1,0:T(8,128)(2,1)}, u32[]{:S(2)}, u32[]{:S(2)}) collective-permute-start(bf16[256,2048]{1,0:T(8,128)(2,1)} %get-tuple-element.24), channel_id=1, source_target_pairs={{0,1},{1,2},{2,3},{3,0},{4,5},{5,6},{6,7},{7,4},{8,9},{9,10},{10,1... | collective-permute-start | bytes 3145736 | tf_op jit(solution)/shard_map/ppermute | solution.py:264
  96.0 53.9 %copy-start.4 = (bf16[128,2048]{1,0:T(8,128)(2,1)}, bf16[128,2048]{1,0:T(8,128)(2,1)S(1)}, u32[]{:S(2)}) copy-start(bf16[128,2048]{1,0:T(8,128)(2,1)S(1)} %all_to_all.44.refs_0_) | copy-start | bytes 1572868
  96.0 11.8 %collective-permute-start.11 = (bf16[2048,128]{1,0:T(8,128)(2,1)}, bf16[2048,128]{1,0:T(8,128)(2,1)S(1)}, u32[]{:S(2)}, u32[]{:S(2)}) collective-permute-start(bf16[2048,128]{1,0:T(8,128)(2,1)} %get-tuple-element.30), channel_id=1, source_target_pairs={{0,8},{4,12},{8,16},{12,20},{16,24},{20,28},{24,0},{28,4},{32,40},... | collective-permute-start | bytes 1572872 | tf_op jit(solution)/shard_map/ppermute | solution.py:277
  97.5 42.4 %collective-permute-start.17 = (bf16[128,2048]{1,0:T(8,128)(2,1)S(1)}, bf16[128,2048]{1,0:T(8,128)(2,1)S(1)}, u32[]{:S(2)}, u32[]{:S(2)}) collective-permute-start(bf16[128,2048]{1,0:T(8,128)(2,1)S(1)} %all_to_all.44.refs_0_), channel_id=1, source_target_pairs={{0,3},{1,0},{2,1},{3,2},{4,7},{5,4},{6,5},{7,6},{8,11},{9,8},{10,9... | collective-permute-start | bytes 1572872 | tf_op jit(solution)/shard_map/ppermute | solution.py:264
  107.8 54.3 %collective-permute-start.19 = (bf16[128,2048]{1,0:T(8,128)(2,1)S(1)}, bf16[128,2048]{1,0:T(8,128)(2,1)}, u32[]{:S(2)}, u32[]{:S(2)}) collective-permute-start(bf16[128,2048]{1,0:T(8,128)(2,1)S(1)} %all_to_all.44.refs_0_), channel_id=1, source_target_pairs={{0,1},{1,2},{2,3},{3,0},{4,5},{5,6},{6,7},{7,4},{8,9},{9,10},{10,1... | collective-permute-start | bytes 1572872 | tf_op jit(solution)/shard_map/ppermute | solution.py:264
  139.9 23.7 %collective-permute-start.6 = (bf16[2048,128]{1,0:T(8,128)(2,1)}, bf16[2048,128]{1,0:T(8,128)(2,1)}, u32[]{:S(2)}, u32[]{:S(2)}) collective-permute-start(bf16[2048,128]{1,0:T(8,128)(2,1)} %collective-permute-done.5), channel_id=1, source_target_pairs={{0,32},{4,36},{8,40},{12,44},{16,48},{20,52},{24,56},{28,60},{32,6... | collective-permute-start | bytes 1572872 | tf_op jit(solution)/shard_map/ppermute | solution.py:277
  140.2 23.5 %collective-permute-start.12 = (bf16[2048,128]{1,0:T(8,128)(2,1)S(1)}, bf16[2048,128]{1,0:T(8,128)(2,1)}, u32[]{:S(2)}, u32[]{:S(2)}) collective-permute-start(bf16[2048,128]{1,0:T(8,128)(2,1)S(1)} %collective-permute-done.11), channel_id=1, source_target_pairs={{0,8},{4,12},{8,16},{12,20},{16,24},{20,28},{24,0},{28,4},{32,40},... | collective-permute-start | bytes 1572872 | tf_op jit(solution)/shard_map/ppermute | solution.py:277
  150.0 41.6 %collective-permute-start.16 = (bf16[256,2048]{1,0:T(8,128)(2,1)S(1)}, bf16[256,2048]{1,0:T(8,128)(2,1)}, u32[]{:S(2)}, u32[]{:S(2)}) collective-permute-start(bf16[256,2048]{1,0:T(8,128)(2,1)S(1)} %bitcast.48), channel_id=1, source_target_pairs={{0,1},{1,2},{2,3},{3,0},{4,5},{5,6},{6,7},{7,4},{8,9},{9,10},{10,1... | collective-permute-start | bytes 3145736 | tf_op jit(solution)/shard_map/ppermute | solution.py:264
  150.8 42.3 %collective-permute-start.22 = (bf16[256,2048]{1,0:T(8,128)(2,1)}, bf16[256,2048]{1,0:T(8,128)(2,1)}, u32[]{:S(2)}, u32[]{:S(2)}) collective-permute-start(bf16[256,2048]{1,0:T(8,128)(2,1)} %get-tuple-element.16), channel_id=1, source_target_pairs={{0,3},{1,0},{2,1},{3,2},{4,7},{5,4},{6,5},{7,6},{8,11},{9,8},{10,9... | collective-permute-start | bytes 3145736 | tf_op jit(solution)/shard_map/ppermute | solution.py:264
  162.1 22.6 %collective-permute-start.18 = (bf16[128,2048]{1,0:T(8,128)(2,1)S(1)}, bf16[128,2048]{1,0:T(8,128)(2,1)S(1)}, u32[]{:S(2)}, u32[]{:S(2)}) collective-permute-start(bf16[128,2048]{1,0:T(8,128)(2,1)S(1)} %collective-permute-done.17.refs_1_), channel_id=1, source_target_pairs={{0,3},{1,0},{2,1},{3,2},{4,7},{5,4},{6,5},{7,6},{8,11},{9,8},{10,9... | collective-permute-start | bytes 1572872 | tf_op jit(solution)/shard_map/ppermute | solution.py:264
  163.6 44.3 %collective-permute-start.30 = (bf16[256,2048]{1,0:T(8,128)(2,1)}, bf16[256,2048]{1,0:T(8,128)(2,1)S(1)}, u32[]{:S(2)}, u32[]{:S(2)}) collective-permute-start(bf16[256,2048]{1,0:T(8,128)(2,1)} %get-tuple-element.23), channel_id=1, source_target_pairs={{0,3},{1,0},{2,1},{3,2},{4,7},{5,4},{6,5},{7,6},{8,11},{9,8},{10,9... | collective-permute-start | bytes 3145736 | tf_op jit(solution)/shard_map/ppermute | solution.py:264
  163.7 49.9 %collective-permute-start.33 = (bf16[256,2048]{1,0:T(8,128)(2,1)}, bf16[256,2048]{1,0:T(8,128)(2,1)}, u32[]{:S(2)}, u32[]{:S(2)}) collective-permute-start(bf16[256,2048]{1,0:T(8,128)(2,1)} %expert.12), channel_id=1, source_target_pairs={{0,1},{1,2},{2,3},{3,0},{4,5},{5,6},{6,7},{7,4},{8,9},{9,10},{10,1... | collective-permute-start | bytes 3145736 | tf_op jit(solution)/shard_map/ppermute | solution.py:264
  184.7 113.5 %collective-permute-start.13 = (bf16[8192,128]{1,0:T(8,128)(2,1)}, bf16[8192,128]{1,0:T(8,128)(2,1)}, u32[]{:S(2)}, u32[]{:S(2)}) collective-permute-start(bf16[8192,128]{1,0:T(8,128)(2,1)} %constant_dynamic-update-slice_fusion.4.near_key), channel_id=1, source_target_pairs={{0,4},{4,0},{8,12},{12,8},{16,20},{20,16},{24,28},{28,24},{32,36},... | collective-permute-start | bytes 6291464 | tf_op jit(solution)/shard_map/ppermute | solution.py:287
  191.6 39.0 %collective-permute-start.24 = (bf16[256,2048]{1,0:T(8,128)(2,1)}, bf16[256,2048]{1,0:T(8,128)(2,1)S(1)}, u32[]{:S(2)}, u32[]{:S(2)}) collective-permute-start(bf16[256,2048]{1,0:T(8,128)(2,1)} %get-tuple-element.18), channel_id=1, source_target_pairs={{0,1},{1,2},{2,3},{3,0},{4,5},{5,6},{6,7},{7,4},{8,9},{9,10},{10,1... | collective-permute-start | bytes 3145736 | tf_op jit(solution)/shard_map/ppermute | solution.py:264
  205.1 39.8 %collective-permute-start.25 = (bf16[256,2048]{1,0:T(8,128)(2,1)}, bf16[256,2048]{1,0:T(8,128)(2,1)}, u32[]{:S(2)}, u32[]{:S(2)}) collective-permute-start(bf16[256,2048]{1,0:T(8,128)(2,1)} %get-tuple-element.19), channel_id=1, source_target_pairs={{0,3},{1,0},{2,1},{3,2},{4,7},{5,4},{6,5},{7,6},{8,11},{9,8},{10,9... | collective-permute-start | bytes 3145736 | tf_op jit(solution)/shard_map/ppermute | solution.py:264
  207.9 90.3 %collective-permute-start.14 = (bf16[8192,128]{1,0:T(8,128)(2,1)}, bf16[8192,128]{1,0:T(8,128)(2,1)}, u32[]{:S(2)}, u32[]{:S(2)}) collective-permute-start(bf16[8192,128]{1,0:T(8,128)(2,1)} %constant_dynamic-update-slice_fusion.15.near_value), channel_id=1, source_target_pairs={{0,4},{4,0},{8,12},{12,8},{16,20},{20,16},{24,28},{28,24},{32,36},... | collective-permute-start | bytes 6291464 | tf_op jit(solution)/shard_map/ppermute | solution.py:287
  220.6 34.6 %all-to-all-start.4 = ((bf16[32,8,2048]{2,1,0:T(8,128)(2,1)}), bf16[32,8,2048]{2,1,0:T(8,128)(2,1)S(1)}, u32[]{:S(2)}, u32[]{:S(2)}) async-start(bf16[32,8,2048]{2,1,0:T(8,128)(2,1)} %bitcast.55), calls=%async_computation.4 | async-start | bytes 2097152 | tf_op jit(solution)/shard_map/all_to_all | solution.py:291
  229.4 15.5 %collective-permute-start.26 = (bf16[128,2048]{1,0:T(8,128)(2,1)S(1)}, bf16[128,2048]{1,0:T(8,128)(2,1)S(1)}, u32[]{:S(2)}, u32[]{:S(2)}) collective-permute-start(bf16[128,2048]{1,0:T(8,128)(2,1)S(1)} %copy-done.20), channel_id=1, source_target_pairs={{0,1},{1,2},{2,3},{3,0},{4,5},{5,6},{6,7},{7,4},{8,9},{9,10},{10,1... | collective-permute-start | bytes 1572872 | tf_op jit(solution)/shard_map/ppermute | solution.py:264
  255.2 33.3 %copy-start.2 = (bf16[32,8,2048]{2,1,0:T(8,128)(2,1)}, bf16[32,8,2048]{2,1,0:T(8,128)(2,1)S(1)}, u32[]{:S(2)}) copy-start(bf16[32,8,2048]{2,1,0:T(8,128)(2,1)S(1)} %all-to-all-done.4) | copy-start | bytes 3145732
  255.2 35.4 %all-to-all-start.5 = ((bf16[32,8,2048]{2,1,0:T(8,128)(2,1)}), bf16[32,8,2048]{2,1,0:T(8,128)(2,1)S(1)}, u32[]{:S(2)}, u32[]{:S(2)}) async-start(bf16[32,8,2048]{2,1,0:T(8,128)(2,1)} %bitcast.56), calls=%async_computation.5 | async-start | bytes 2097152 | tf_op jit(solution)/shard_map/all_to_all | solution.py:291
  263.4 17.0 %collective-permute-start.23 = (bf16[128,2048]{1,0:T(8,128)(2,1)}, bf16[128,2048]{1,0:T(8,128)(2,1)S(1)}, u32[]{:S(2)}, u32[]{:S(2)}) collective-permute-start(bf16[128,2048]{1,0:T(8,128)(2,1)} %get-tuple-element.17), channel_id=1, source_target_pairs={{0,3},{1,0},{2,1},{3,2},{4,7},{5,4},{6,5},{7,6},{8,11},{9,8},{10,9... | collective-permute-start | bytes 1572872 | tf_op jit(solution)/shard_map/ppermute | solution.py:264
  264.9 15.5 %collective-permute-start.27 = (bf16[128,2048]{1,0:T(8,128)(2,1)}, bf16[128,2048]{1,0:T(8,128)(2,1)S(1)}, u32[]{:S(2)}, u32[]{:S(2)}) collective-permute-start(bf16[128,2048]{1,0:T(8,128)(2,1)} %get-tuple-element.21), channel_id=1, source_target_pairs={{0,1},{1,2},{2,3},{3,0},{4,5},{5,6},{6,7},{7,4},{8,9},{9,10},{10,1... | collective-permute-start | bytes 1572872 | tf_op jit(solution)/shard_map/ppermute | solution.py:264
  265.6 14.0 %collective-permute-start = (bf16[256,256]{1,0:T(8,128)(2,1)}, bf16[256,256]{1,0:T(8,128)(2,1)S(1)}, u32[]{:S(2)}, u32[]{:S(2)}) collective-permute-start(bf16[256,256]{1,0:T(8,128)(2,1)} %get-tuple-element.29), channel_id=1, source_target_pairs={{0,124},{4,120},{8,116},{12,112},{16,108},{20,104},{24,100},{28,96... | collective-permute-start | bytes 393224 | tf_op jit(solution)/shard_map/ppermute | solution.py:269
  290.6 45.4 %copy-start.3 = (bf16[32,8,2048]{2,1,0:T(8,128)(2,1)}, bf16[32,8,2048]{2,1,0:T(8,128)(2,1)S(1)}, u32[]{:S(2)}) copy-start(bf16[32,8,2048]{2,1,0:T(8,128)(2,1)S(1)} %all-to-all-done.5) | copy-start | bytes 3145732
  290.6 59.7 %all-to-all-start.2 = ((bf16[32,4,2048]{2,1,0:T(4,128)(2,1)}), bf16[32,4,2048]{2,1,0:T(4,128)(2,1)S(1)}, u32[]{:S(2)}, u32[]{:S(2)}) async-start(bf16[32,4,2048]{2,1,0:T(4,128)(2,1)} %all_to_all.48), calls=%async_computation.2 | async-start | bytes 1048576 | tf_op jit(solution)/shard_map/all_to_all | solution.py:291
  298.2 39.0 %copy-start.17 = (s32[128,4]{0,1:T(4,128)S(1)}, s32[128,4]{0,1:T(4,128)}, u32[]{:S(2)}) copy-start(s32[128,4]{0,1:T(4,128)} %param.18) | copy-start | bytes 6148
  298.2 39.7 %copy-start.18 = (f32[128,4]{0,1:T(4,128)S(1)}, f32[128,4]{0,1:T(4,128)}, u32[]{:S(2)}) copy-start(f32[128,4]{0,1:T(4,128)} %param.19) | copy-start | bytes 6148
  337.0 8.9 %collective-permute-start.15 = (bf16[256,256]{1,0:T(8,128)(2,1)S(1)}, bf16[256,256]{1,0:T(8,128)(2,1)S(1)}, u32[]{:S(2)}, u32[]{:S(2)}) collective-permute-start(bf16[256,256]{1,0:T(8,128)(2,1)S(1)} %get-tuple-element.27), channel_id=1, source_target_pairs={{0,124},{4,120},{8,116},{12,112},{16,108},{20,104},{24,100},{28,96... | collective-permute-start | bytes 393224 | tf_op jit(solution)/shard_map/ppermute | solution.py:269
  (11 other events, 93.7 us)
